TPU v7x, 32 devices: a whole 2x2x4 slice. The times are simulated.
32 devices in a mesh: ep: 4 (over y, x), tp: 8 (over z, core).
Axes of the slice: x: 2, y: 2, z: 4, core: 2. Of those that a mesh axis runs over, the one named last changes fastest.
Arguments:
- tokens: bfloat16 [1024, 4096], P('ep'), may hold values from -6 to 6
- cotangent: bfloat16 [1024, 4096], P('ep'), may hold values from -6 to 6
- routing: int32 [1024, 2], P('ep'), may hold values from 0 to 3, all different within a row; in each aligned block of 256 rows (0 to 255, 256 to 511, ...) at most 160 rows name the same one
- group_gate: float32 [1024], P('ep'), may hold values from 0.2 to 1
- inner_gate: float32 [1024, 2], P('ep'), may hold values from 0.1 to 0.9
- w_gate: bfloat16 [4, 4096, 2048], P('ep', None, 'tp'), may hold values from -0.09375 to 0.09375
- w_up: bfloat16 [4, 4096, 2048], P('ep', None, 'tp'), may hold values from -0.09375 to 0.09375
- w_down: bfloat16 [4, 2048, 4096], P('ep', 'tp'), may hold values from -0.125 to 0.125
Outputs:
- token_grad: bfloat16 [1024, 4096], P('ep', 'tp')
- group_grad: float32 [1024], P('ep')
- inner_grad: float32 [1024, 2], P('ep')
- gate_weight_grad: bfloat16 [4, 4096, 2048], P('ep', None, 'tp')
- up_weight_grad: bfloat16 [4, 4096, 2048], P('ep', None, 'tp')
- down_weight_grad: bfloat16 [4, 2048, 4096], P('ep', 'tp')
Inputs may be any that keep to these rules, and one draw needn't show every extreme that they name: `routing`: each row names 2 different experts. Among the rows of one device (aligned blocks of 256 rows) no expert is named more than 160 times, and in every draw some expert is named exactly 160 times in some block.
All inputs are finite; a program needn't handle non-finite values.
Results may differ from a plain program's by a relative error of at most 0.02.
Values may be sent and summed in bfloat16 or wider, within the bound.
A program may use at most 128 MiB of HBM per device.

v0:
```python
import functools

import jax
import jax.numpy as jnp
from jax import lax
from jax.experimental import pallas as pl
from jax.experimental.pallas import tpu as pltpu
from jax.sharding import PartitionSpec as P

LANES = 128
BF16 = jnp.bfloat16
F32 = jnp.float32


def peer_of(me, d, n):
    if n & (n - 1):
        return lax.rem(2 * n + d - me, n)
    out, bit = me, 1
    while bit < n:
        if d & bit:
            out = out + bit * (1 - 2 * lax.rem(me // bit, 2))
        bit *= 2
    return out


def barrier(partners):
    sem = pltpu.get_barrier_semaphore()
    for ep, tp in partners:
        pl.semaphore_signal(
            sem, inc=1, device_id=(ep, tp), device_id_type=pl.DeviceIdType.MESH
        )
    pl.semaphore_wait(sem, len(partners))


def remote(src, dst, send, recv, ep, tp):
    return pltpu.make_async_remote_copy(
        src_ref=src,
        dst_ref=dst,
        send_sem=send,
        recv_sem=recv,
        device_id=(ep, tp),
        device_id_type=pl.DeviceIdType.MESH,
    )


def dispatch_kernel(n_ep, n_tp, xs, gs, cs, x_out, g_out, c_out, send, recv, c_send, c_recv, stage, local):
    ep, tp = lax.axis_index("ep"), lax.axis_index("tp")
    core = lax.rem(tp, 2)
    z = tp // 2
    sibling = tp + 1 - 2 * core
    odd = lax.rem(z, 2)
    across = tp + 2 - 4 * odd
    half = xs.shape[2] // 2
    blocks = half // LANES
    lone = blocks * 3 // 8 * LANES
    both = half - 2 * lone
    base = core * half
    peers = [peer_of(ep, d, n_ep) for d in range(1, n_ep)]
    barrier([(p, tp) for p in peers] + [(ep, sibling), (ep, across)])

    def cols(start, width):
        return pl.ds(pl.multiple_of(start, LANES), width)

    mine = cols(base + odd * (lone + both), lone)
    theirs = cols(base + (1 - odd) * (lone + both), lone)
    shared = cols(base + lone, both)

    pairs = ((xs, x_out), (gs, g_out))
    started, direct = [], {}
    for d, p in enumerate(peers):
        copy = remote(cs.at[p], c_out.at[ep], c_send.at[d], c_recv.at[d], p, tp)
        copy.start()
        started.append(copy)
    for kind, part in ((0, mine), (1, shared)):
        for a, (src, dst) in enumerate(pairs):
            for d, p in enumerate(peers):
                copy = remote(
                    src.at[p, :, part], dst.at[ep, :, part],
                    send.at[a, d, kind], recv.at[a, d, kind], p, tp,
                )
                copy.start()
                direct[a, kind, d] = copy
    loads = []
    for a, (src, dst) in enumerate(pairs):
        load = pltpu.make_async_copy(src.at[ep], stage.at[a], local.at[a])
        load.start()
        loads.append(load)
    load = pltpu.make_async_copy(cs.at[ep], stage_c(c_out, ep), local.at[4])
    load.start()
    stores = [load]
    for a, (src, dst) in enumerate(pairs):
        loads[a].wait()
        store = pltpu.make_async_copy(stage.at[a], dst.at[ep], local.at[2 + a])
        store.start()
        stores.append(store)

    forwards = []
    for kind, part in ((0, mine), (1, shared)):
        for a, (src, dst) in enumerate(pairs):
            for d, p in enumerate(peers):
                direct[a, kind, d].wait_recv()
                if kind == 0:
                    copy = remote(
                        dst.at[p, :, part], dst.at[p, :, part],
                        send.at[a, d, 2], recv.at[a, d, 2], ep, across,
                    )
                    copy.start()
                    forwards.append(copy)
                    direct[a, 2, d] = remote(
                        dst.at[p, :, theirs], dst.at[p, :, theirs],
                        send.at[a, d, 2], recv.at[a, d, 2], ep, across,
                    )
                copy = remote(
                    dst.at[p, :, part], dst.at[p, :, part],
                    send.at[a, d, 3 + kind], recv.at[a, d, 3 + kind], ep, sibling,
                )
                copy.start()
                forwards.append(copy)
    for a, (src, dst) in enumerate(pairs):
        for d, p in enumerate(peers):
            direct[a, 2, d].wait_recv()
            copy = remote(
                dst.at[p, :, theirs], dst.at[p, :, theirs],
                send.at[a, d, 5], recv.at[a, d, 5], ep, sibling,
            )
            copy.start()
            forwards.append(copy)
    for a, (src, dst) in enumerate(pairs):
        for d, p in enumerate(peers):
            for kind, offset, width in (
                (3, odd * (lone + both), lone),
                (4, lone, both),
                (5, (1 - odd) * (lone + both), lone),
            ):
                part = cols((1 - core) * half + offset, width)
                remote(
                    dst.at[p, :, part], dst.at[p, :, part],
                    send.at[a, d, kind], recv.at[a, d, kind], ep, sibling,
                ).wait_recv()
    for copy in started:
        copy.wait()
    for key, copy in direct.items():
        if key[1] != 2:
            copy.wait_send()
    for copy in forwards:
        copy.wait_send()
    for store in stores:
        store.wait()


def stage_c(c_out, ep):
    return c_out.at[ep]


def dispatch(n_ep, n_tp, xs, gs, cs):
    any_spec = pl.BlockSpec(memory_space=pl.ANY)
    return pl.pallas_call(
        functools.partial(dispatch_kernel, n_ep, n_tp),
        out_shape=(
            jax.ShapeDtypeStruct(xs.shape, xs.dtype),
            jax.ShapeDtypeStruct(gs.shape, gs.dtype),
            jax.ShapeDtypeStruct(cs.shape, cs.dtype),
        ),
        in_specs=[any_spec] * 3,
        out_specs=(any_spec,) * 3,
        scratch_shapes=[
            pltpu.SemaphoreType.DMA((2, n_ep - 1, 6)),
            pltpu.SemaphoreType.DMA((2, n_ep - 1, 6)),
            pltpu.SemaphoreType.DMA((n_ep - 1,)),
            pltpu.SemaphoreType.DMA((n_ep - 1,)),
            pltpu.VMEM((2,) + xs.shape[1:], xs.dtype),
            pltpu.SemaphoreType.DMA((5,)),
        ],
        compiler_params=pltpu.CompilerParams(collective_id=0, has_side_effects=True),
    )(xs, gs, cs)


def return_kernel(n_ep, n_tp, ggu, wg, wu, pick, hid, weight, sc, x_hbm, g_hbm,
                  out, sc_out, gate_out, up_out, down_out,
                  first, first_in, second, second_in, third, third_in,
                  xv, gv, gate_v, up_v, down_v,
                  s1, r1, s2, r2, s3, r3, ss, rs, sl, fetch, flush):
    ep, tp = lax.axis_index("ep"), lax.axis_index("tp")
    core = lax.rem(tp, 2)
    z = tp // 2
    nz = n_tp // 2
    sibling = tp + 1 - 2 * core
    width = out.shape[1]
    units = wg.shape[1]
    cap = second.shape[2]
    peers = [peer_of(ep, d, n_ep) for d in range(1, n_ep)]
    everyone = [(p, tp) for p in peers]
    everyone += [(ep, lax.rem(tp + k, n_tp)) for k in range(1, n_tp)]
    score_to = [(p, lax.rem(tp + k, n_tp)) for p in [ep] + peers for k in range(n_tp)][1:]
    fetches = [
        pltpu.make_async_copy(x_hbm, xv, fetch.at[0]),
        pltpu.make_async_copy(g_hbm, gv, fetch.at[1]),
    ]
    for copy in fetches:
        copy.start()
    barrier(score_to)

    sends = []
    for i, (p, t) in enumerate(score_to):
        copy = remote(sc.at[p], sc_out.at[ep, tp], ss.at[i], rs.at[i], p, t)
        copy.start()
        sends.append(copy)
    own_score = pltpu.make_async_copy(sc.at[ep], sc_out.at[ep, tp], sl)
    own_score.start()

    def partial(share):
        rows = pl.ds(pl.multiple_of(share * width, width), width)
        dims = (((1,), (1,)), ((), ()))
        return lax.dot_general(
            ggu[:, :units], wg[rows, :], dims, preferred_element_type=F32
        ) + lax.dot_general(ggu[:, units:], wu[rows, :], dims, preferred_element_type=F32)

    def tile(t):
        return pl.ds(pl.multiple_of(t * width, width), width)

    def gate_up_tiles(lo, hi):
        def step(t, carry):
            both = lax.dot_general(
                xv[:, tile(t)], ggu[...], (((0,), (0,)), ((), ())), preferred_element_type=F32
            ).astype(BF16)
            gate_v[tile(t), :] = both[:, :units]
            up_v[tile(t), :] = both[:, units:]
            return carry

        lax.fori_loop(lo, hi, step, 0)

    def early():
        fetches[0].wait()
        gate_up_tiles(0, n_tp // 2)

    def middle():
        gate_up_tiles(n_tp // 2, n_tp)
        for k, (src, dst) in enumerate(((gate_v, gate_out), (up_v, up_out))):
            copy = pltpu.make_async_copy(src, dst, flush.at[k])
            copy.start()
            flushes.append(copy)

    def late():
        fetches[1].wait()
        hidden_t = hid[...].T

        def step(t, carry):
            scaled = (weight[...] * gv[:, tile(t)].astype(F32)).astype(BF16)
            down_v[:, tile(t)] = jnp.dot(
                hidden_t, scaled, preferred_element_type=F32
            ).astype(BF16)
            return carry

        lax.fori_loop(0, n_tp, step, 0)
        copy = pltpu.make_async_copy(down_v, down_out, flush.at[2])
        copy.start()
        flushes.append(copy)

    flushes = []
    work = [early, middle, late]
    order = [lax.rem(z + dz, nz) for dz in range(nz - 1, -1, -1)]
    halves = []
    for i, zz in enumerate(order):
        first[i] = partial(2 * zz + 1 - core).astype(BF16)
        copy = remote(first.at[i], first_in.at[i], s1.at[i], r1.at[i], ep, sibling)
        copy.start()
        halves.append(copy)
    moves = {}
    for i, zz in enumerate(order):
        total = partial(2 * zz + core)
        halves[i].wait_recv()
        total = total + first_in[i].astype(F32)
        second[i] = total.astype(BF16).reshape(second.shape[1:])
        for d, p in enumerate(peers):
            copy = remote(
                second.at[i, p], second_in.at[i, ep], s2.at[i, d], r2.at[i, d], p, tp
            )
            copy.start()
            moves[i, d] = copy
    last = []
    for i, zz in enumerate(order):
        for job in work[i:] if i == nz - 1 else work[i : i + 1]:
            job()
        for d, p in enumerate(peers):
            moves[i, d].wait_recv()
        second_in[i, ep] = second[i, ep]
        rows = second_in[i].reshape(n_ep * cap, width)
        summed = jnp.dot(pick[...], rows, preferred_element_type=F32)
        third[i] = summed.astype(BF16)
        if i < nz - 1:
            copy = remote(
                third.at[i], third_in.at[i], s3.at[i], r3.at[i], ep, 2 * zz + core
            )
            copy.start()
            last.append(copy)
    total = third[nz - 1].astype(F32)
    for i in range(nz - 1):
        last[i].wait_recv()
        total = total + third_in[i].astype(F32)
    out[...] = total.astype(BF16)
    for copy in halves + list(moves.values()) + last:
        copy.wait_send()
    for copy in sends:
        copy.wait()
    own_score.wait()
    for copy in flushes:
        copy.wait()


def give_back(n_ep, n_tp, ggu, wg, wu, pick, hid, weight, sc, rows_in, cot_rows):
    vmem = pl.BlockSpec(memory_space=pltpu.VMEM)
    any_spec = pl.BlockSpec(memory_space=pl.ANY)
    rows, nz = ggu.shape[0], n_tp // 2
    width = wg.shape[0] // n_tp
    tokens = pick.shape[0]
    cap = rows // n_ep
    dma = pltpu.SemaphoreType.DMA
    others = n_ep * n_tp - 1
    return pl.pallas_call(
        functools.partial(return_kernel, n_ep, n_tp),
        out_shape=(
            jax.ShapeDtypeStruct((tokens, width), BF16),
            jax.ShapeDtypeStruct((n_ep, n_tp) + sc.shape[1:], F32),
            jax.ShapeDtypeStruct(wg.shape, BF16),
            jax.ShapeDtypeStruct(wu.shape, BF16),
            jax.ShapeDtypeStruct(wg.shape[::-1], BF16),
        ),
        in_specs=[vmem] * 6 + [any_spec] * 3,
        out_specs=(vmem,) + (any_spec,) * 4,
        scratch_shapes=[
            pltpu.VMEM((nz, rows, width), BF16),
            pltpu.VMEM((nz, rows, width), BF16),
            pltpu.VMEM((nz, n_ep, cap, width), BF16),
            pltpu.VMEM((nz, n_ep, cap, width), BF16),
            pltpu.VMEM((nz, tokens, width), BF16),
            pltpu.VMEM((nz, tokens, width), BF16),
            pltpu.VMEM(rows_in.shape, BF16),
            pltpu.VMEM(cot_rows.shape, BF16),
            pltpu.VMEM(wg.shape, BF16),
            pltpu.VMEM(wu.shape, BF16),
            pltpu.VMEM(wg.shape[::-1], BF16),
            dma((nz,)), dma((nz,)),
            dma((nz, n_ep - 1)), dma((nz, n_ep - 1)),
            dma((nz,)), dma((nz,)),
            dma((others,)), dma((others,)),
            dma,
            dma((2,)),
            dma((3,)),
        ],
        compiler_params=pltpu.CompilerParams(
            collective_id=1, has_side_effects=True, vmem_limit_bytes=56 * 1024 * 1024
        ),
    )(ggu, wg, wu, pick, hid, weight, sc, rows_in, cot_rows)


def per_device(tokens, cotangent, routing, group_gate, inner_gate, w_gate, w_up, w_down):
    n_ep, n_tp = lax.axis_size("ep"), lax.axis_size("tp")
    tok_rows, model_width = tokens.shape
    top_k = routing.shape[1]
    cap = tok_rows * top_k * 5 // (4 * n_ep)
    rows = n_ep * cap
    experts = jnp.arange(n_ep, dtype=jnp.int32)
    route_t = routing.T
    names = jnp.sum((route_t[:, None, :] == experts[None, :, None]).astype(F32), axis=0)
    place = jnp.arange(tok_rows)
    before = (place[:, None] < place[None, :]).astype(BF16)
    rank = jnp.dot(names.astype(BF16), before, preferred_element_type=F32).astype(jnp.int32)
    slot_t = jnp.sum(
        jnp.where(
            route_t[:, None, :] == experts[None, :, None],
            experts[None, :, None] * cap + rank[None],
            0,
        ),
        axis=1,
    )
    slots = jnp.arange(rows, dtype=jnp.int32)
    hits = slots[:, None, None] == slot_t[None]
    put = jnp.any(hits, axis=1).astype(BF16)
    combine = (group_gate[:, None] * inner_gate).T
    weight = jnp.sum(jnp.where(hits, combine[None], 0.0), axis=(1, 2))
    pad = -cap % LANES
    send_weight = jnp.pad(weight.reshape(n_ep, 1, cap), ((0, 0), (0, 0), (0, pad)))

    def placed(source):
        return jnp.dot(put, source, preferred_element_type=F32).astype(BF16).reshape(
            n_ep, cap, model_width
        )

    rows_in, cot_rows, weight_in = dispatch(
        n_ep, n_tp, placed(tokens), placed(cotangent), send_weight
    )
    rows_in = rows_in.reshape(rows, model_width)
    cot_rows = cot_rows.reshape(rows, model_width)
    row_weight = weight_in[:, 0, :cap].reshape(rows)

    gate_weight, up_weight, down_weight = w_gate[0], w_up[0], w_down[0]
    gate_pre = jnp.dot(rows_in, gate_weight, preferred_element_type=F32)
    up_pre = jnp.dot(rows_in, up_weight, preferred_element_type=F32)
    sigmoid_gate = jax.nn.sigmoid(gate_pre)
    silu_gate = gate_pre * sigmoid_gate
    hidden = (silu_gate * up_pre).astype(BF16)
    grad_hidden = lax.dot_general(
        cot_rows, down_weight, (((1,), (1,)), ((), ())), preferred_element_type=F32
    )
    partial_scores = jnp.sum(grad_hidden * hidden.astype(F32), axis=1)
    weighted = row_weight[:, None] * grad_hidden
    grad_gate_in = (
        weighted * up_pre * sigmoid_gate * (1.0 + gate_pre * (1.0 - sigmoid_gate))
    ).astype(BF16)
    grad_up_in = (weighted * silu_gate).astype(BF16)
    send_score = jnp.pad(
        partial_scores.reshape(n_ep, 1, cap), ((0, 0), (0, 0), (0, pad))
    )
    token_grad, all_scores, gate_grad, upper_grad, down_grad = give_back(
        n_ep, n_tp, jnp.concatenate([grad_gate_in, grad_up_in], axis=1),
        gate_weight, up_weight, put.T, hidden, row_weight[:, None], send_score,
        rows_in, cot_rows,
    )
    scores = jnp.sum(all_scores[:, :, 0, :cap], axis=1).reshape(rows)
    score_t = jnp.sum(jnp.where(hits, scores[:, None, None], 0.0), axis=0)
    score_of = score_t.T
    inner_grad = group_gate[:, None] * score_of
    group_grad = jnp.sum(inner_gate * score_of, axis=1)
    return (
        token_grad,
        group_grad,
        inner_grad,
        gate_grad[None],
        upper_grad[None],
        down_grad[None],
    )


def solution(mesh):
    return jax.shard_map(
        per_device,
        mesh=mesh,
        in_specs=(
            P("ep", None),
            P("ep", None),
            P("ep", None),
            P("ep"),
            P("ep", None),
            P("ep", None, "tp"),
            P("ep", None, "tp"),
            P("ep", "tp", None),
        ),
        out_specs=(
            P("ep", "tp"),
            P("ep"),
            P("ep", None),
            P("ep", None, "tp"),
            P("ep", None, "tp"),
            P("ep", "tp", None),
        ),
        check_vma=False,
    )
```

profile of v0, /device:TPU:0, one launch (start us, length us, event | category | flops | bytes accessed | tf_op | source)
XLA Modules:
  0.0 131.2 jit_solution(11678975112914654358)
XLA Ops:
  0.6 0.0 copy-start
  0.6 0.8 convert_reduce_fusion
  1.5 0.1 fusion.3
  1.6 0.7 select_reduce_fusion.2
  2.4 0.2 fusion.2
  2.6 0.0 copy-done
  2.6 0.0 copy-start.5
  2.6 3.9 %convolution_convert_fusion.1 = bf16[640,4096]{1,0:T(8,128)(2,1)} fusion(pred[640,256]{1,0:T(8,128)(4,1)S(1)} %fusion.2, bf16[256,4096]{1,0:T(8,128)(2,1)S(1)} %copy-done), kind=kOutput, calls=%fused_computation.1 | convolution fusion | flops 1344798720 | bytes 7503872 | tf_op jit(solution)/shard_map/dot_general | solution.py:385
  6.5 0.0 copy-done.5
  6.5 0.0 copy-start.6
  6.5 0.0 copy-start.8
  6.5 3.8 %convolution_convert_fusion = bf16[640,4096]{1,0:T(8,128)(2,1)} fusion(pred[640,256]{1,0:T(8,128)(4,1)S(1)} %fusion.2, bf16[256,4096]{1,0:T(8,128)(2,1)S(1)} %copy-done.5), kind=kOutput, calls=%fused_computation | convolution fusion | flops 1344798720 | bytes 7503872 | tf_op jit(solution)/shard_map/dot_general | solution.py:385
  10.3 0.0 copy-done.6
  10.3 0.0 copy-done.8
  10.3 0.2 select_reduce_fusion.1
  10.5 0.1 reshape.47
  10.6 0.6 pad.7.cs
  11.2 46.1 %shard_map.127 = (bf16[4,160,4096]{2,1,0:T(8,128)(2,1)}, bf16[4,160,4096]{2,1,0:T(8,128)(2,1)}, f32[4,1,256]{2,1,0:T(1,128)}) custom-call(bf16[4,160,4096]{2,1,0:T(8,128)(2,1)} %bitcast.36, bf16[4,160,4096]{2,1,0:T(8,128)(2,1)} %bitcast.37, f32[4,1,256]{2,1,0:T(1,128)} %pad.7.cs), custom_call_target="tpu_custom_call" | custom-call | tf_op jit(solution)/shard_map/pallas_call | solution.py:157
  57.3 0.0 copy-start.1
  57.3 0.0 copy-start.2
  57.3 4.8 %fusion.7 = f32[640,256]{1,0:T(8,128)S(1)} fusion(bf16[640,4096]{1,0:T(8,128)(2,1)} %bitcast.38, bf16[1,4096,256]{2,1,0:T(8,128)(2,1)} %param.13), kind=kOutput, calls=%fused_computation.30 | convolution fusion | flops 1342177280 | bytes 7995392 | tf_op jit(solution)/shard_map/dot_general | solution.py:397
  62.1 0.0 copy-done.1
  62.1 0.5 copy-done.2
  62.6 0.0 copy-start.7
  62.6 2.4 %fusion.9 = f32[640,256]{1,0:T(8,128)} fusion(bf16[640,4096]{1,0:T(8,128)(2,1)S(1)} %bitcast.40, bf16[1,4096,256]{2,1,0:T(8,128)(2,1)S(1)} %copy-done.2), kind=kOutput, calls=%fused_computation.32 | convolution fusion | flops 1342177280 | bytes 7995392 | tf_op jit(solution)/shard_map/dot_general | solution.py:398
  64.9 0.0 copy-done.7
  65.0 0.1 mul.62
  65.0 5.7 %multiply_reduce_fusion = (f32[640]{0:T(1024)S(1)}, bf16[640,256]{1,0:T(8,128)(2,1)}, bf16[640,256]{1,0:T(8,128)(2,1)S(1)}, bf16[640,256]{1,0:T(8,128)(2,1)S(1)}) fusion(f32[640,256]{1,0:T(8,128)} %fusion.9, f32[640,256]{1,0:T(8,128)S(1)} %fusion.7, f32[640]{0:T(1024)S(1)} %mul.62, bf16[640,4096]{1,0:T(8,128)(2,1)} %bitcast.41, bf16[1,256,4096]{2,1,0:T(8,128)(2,1)} %param.15), kind=kOutput, calls=%fused_computation.11 | convolution fusion | flops 1345289600 | bytes 9638912 | tf_op jit(solution)/shard_map/dot_general | solution.py:402
  70.8 0.9 pad_maximum_fusion.ggu
  71.7 0.1 reshape.50
  71.7 0.6 pad.8.sc
  72.3 1.0 broadcast_in_dim_reshape_squeeze.5.weight
  73.3 0.3 copy.34
  73.6 0.8 convert_bitcast_fusion.pick
  74.3 46.0 %shard_map.128 = (bf16[256,512]{1,0:T(8,128)(2,1)}, f32[4,8,1,256]{3,2,1,0:T(1,128)}, bf16[4096,256]{1,0:T(8,128)(2,1)}, bf16[4096,256]{1,0:T(8,128)(2,1)}, bf16[256,4096]{1,0:T(8,128)(2,1)}) custom-call(bf16[640,512]{1,0:T(8,128)(2,1)} %pad_maximum_fusion.ggu, bf16[4096,256]{1,0:T(8,128)(2,1)} %bitcast.44, bf16[4096,256]{1,0:T(8,128)(2,1)} %bitcast.43, ...), custom_call_target="tpu_custom_call" | custom-call | tf_op jit(solution)/shard_map/pallas_call | solution.py:319
  120.4 0.8 slice_reduce_fusion
  121.2 0.1 broadcast_in_dim.62
  121.2 0.3 select_reduce_fusion
  121.5 1.1 bitcast_multiply_fusion
  122.6 1.7 %copy.45 = bf16[256,512]{1,0:T(8,128)(2,1)} copy(bf16[256,512]{1,0:T(8,128)(2,1)} %get-tuple-element.34) | data formatting | bytes 524288
  124.3 0.0 copy-start.4
  124.3 3.2 %copy.46 = bf16[1,4096,256]{2,1,0:T(8,128)(2,1)} copy(bf16[1,4096,256]{2,1,0:T(8,128)(2,1)} %bitcast.47) | data formatting | bytes 4194304
  127.5 0.0 copy-done.4
  127.5 0.0 copy-start.3
  127.5 1.3 %copy.47 = bf16[1,4096,256]{2,1,0:T(8,128)(2,1)} copy(bf16[1,4096,256]{2,1,0:T(8,128)(2,1)S(1)} %bitcast.46) | data formatting | bytes 4194304
  128.8 1.0 copy-done.3
  129.9 1.3 %copy.48 = bf16[1,256,4096]{2,1,0:T(8,128)(2,1)} copy(bf16[1,256,4096]{2,1,0:T(8,128)(2,1)S(1)} %bitcast.45) | data formatting | bytes 4194304
  (3 shorter events, 0.0 us)
Async XLA Ops:
  0.6 2.0 %copy-start = (bf16[256,4096]{1,0:T(8,128)(2,1)S(1)}, bf16[256,4096]{1,0:T(8,128)(2,1)}, u32[]{:S(2)}) copy-start(bf16[256,4096]{1,0:T(8,128)(2,1)} %param.8) | copy-start | bytes 6291460
  2.6 3.9 %copy-start.5 = (bf16[256,4096]{1,0:T(8,128)(2,1)S(1)}, bf16[256,4096]{1,0:T(8,128)(2,1)}, u32[]{:S(2)}) copy-start(bf16[256,4096]{1,0:T(8,128)(2,1)} %param.9) | copy-start | bytes 6291460
  6.5 3.8 %copy-start.6 = (f32[256,2]{0,1:T(2,128)S(1)}, f32[256,2]{0,1:T(2,128)}, u32[]{:S(2)}) copy-start(f32[256,2]{0,1:T(2,128)} %param.12) | copy-start | bytes 6148
  6.5 3.8 %copy-start.8 = (f32[256]{0:T(256)S(1)}, f32[256]{0:T(256)}, u32[]{:S(2)}) copy-start(f32[256]{0:T(256)} %param.11) | copy-start | bytes 3076
  57.3 4.8 %copy-start.1 = (bf16[4,160,4096]{2,1,0:T(8,128)(2,1)S(1)}, bf16[4,160,4096]{2,1,0:T(8,128)(2,1)}, u32[]{:S(2)}) copy-start(bf16[4,160,4096]{2,1,0:T(8,128)(2,1)} %get-tuple-element.16) | copy-start | bytes 15728644
  57.3 5.3 %copy-start.2 = (bf16[1,4096,256]{2,1,0:T(8,128)(2,1)S(1)}, bf16[1,4096,256]{2,1,0:T(8,128)(2,1)}, u32[]{:S(2)}) copy-start(bf16[1,4096,256]{2,1,0:T(8,128)(2,1)} %param.14) | copy-start | bytes 6291460
  62.6 2.4 %copy-start.7 = (f32[4,1,256]{2,1,0:T(1,128)S(1)}, f32[4,1,256]{2,1,0:T(1,128)}, u32[]{:S(2)}) copy-start(f32[4,1,256]{2,1,0:T(1,128)} %get-tuple-element.14) | copy-start | bytes 12292
  124.3 3.2 %copy-start.4 = (bf16[4096,256]{1,0:T(8,128)(2,1)S(1)}, bf16[4096,256]{1,0:T(8,128)(2,1)}, u32[]{:S(2)}) copy-start(bf16[4096,256]{1,0:T(8,128)(2,1)} %get-tuple-element.20) | copy-start | bytes 6291460
  127.5 2.3 %copy-start.3 = (bf16[256,4096]{1,0:T(8,128)(2,1)S(1)}, bf16[256,4096]{1,0:T(8,128)(2,1)}, u32[]{:S(2)}) copy-start(bf16[256,4096]{1,0:T(8,128)(2,1)} %get-tuple-element.21) | copy-start | bytes 6291460
where the time goes:
time: 132 us; the launch traced here: 131 us
  Pallas kernels  92.1 us (70%)
  matrix products  20.7 us (16%)
  local copies, waits for them, and re-layouts  11.8 us (9%)
  other arithmetic  5.85 us (4%)
    pallas_call x1, Pallas kernels, dispatch(): pl.pallas_call(functools.partial(dispatch_kernel, n_ep, n_tp), out_shape=...  46.1 us
    pallas_call x1, Pallas kernels, give_back(): pl.pallas_call(functools.partial(return_kernel, n_ep, n_tp), out_shape=(j...  46 us
    unnamed x22, local copies, waits for them, and re-layouts  9.03 us
    dot_general x2, matrix products, placed(): jnp.dot(put, source, preferred_element_type=F32).astype(BF16)  7.68 us
    dot_general x1, matrix products, per_device(): lax.dot_general(cot_rows, down_weight, (((1,), (1,)), ((), ())), preferre...  5.72 us
    dot_general x1, matrix products, per_device(): gate_pre = jnp.dot(rows_in, gate_weight, preferred_element_type=F32)  4.81 us

commit v1 on v0

v1 whole, which is shorter than its diff:
```python
import functools

import jax
import jax.numpy as jnp
from jax import lax
from jax.experimental import pallas as pl
from jax.experimental.pallas import tpu as pltpu
from jax.sharding import PartitionSpec as P

LANES = 128
STEPS = 4
BF16 = jnp.bfloat16
F32 = jnp.float32


def peer_of(me, d, n):
    if n & (n - 1):
        return lax.rem(2 * n + d - me, n)
    out, bit = me, 1
    while bit < n:
        if d & bit:
            out = out + bit * (1 - 2 * lax.rem(me // bit, 2))
        bit *= 2
    return out


def barrier(partners):
    sem = pltpu.get_barrier_semaphore()
    for ep, tp in partners:
        pl.semaphore_signal(
            sem, inc=1, device_id=(ep, tp), device_id_type=pl.DeviceIdType.MESH
        )
    return lambda: pl.semaphore_wait(sem, len(partners))


def remote(src, dst, send, recv, ep, tp):
    return pltpu.make_async_remote_copy(
        src_ref=src,
        dst_ref=dst,
        send_sem=send,
        recv_sem=recv,
        device_id=(ep, tp),
        device_id_type=pl.DeviceIdType.MESH,
    )


def dot_nt(a, b):
    return lax.dot_general(a, b, (((1,), (1,)), ((), ())), preferred_element_type=F32)


def layer_kernel(n_ep, n_tp, cap, route, gates, inner, tok_hbm, cot_hbm, wg_hbm, wu_hbm, wd_hbm,
                 out, group_out, inner_out, gate_out, up_out, down_out,
                 toks, sends, rows_v, wg, wu, wd, tab, put, pick,
                 cs, c_in, square, sc_in, tot, tot_in,
                 acc_g, acc_u, acc_h, ggu, hid,
                 first, first_in, second, second_in, across_v, across_in, own_total, third, third_in,
                 local, drain, recv, sib_recv, c_s, c_r, sc_s, sc_r, tot_s, tot_r,
                 s1, r1, s2, r2, s3, r3, sa, ra):
    ep, tp = lax.axis_index("ep"), lax.axis_index("tp")
    core = lax.rem(tp, 2)
    z = tp // 2
    nz = n_tp // 2
    sibling = tp + 1 - 2 * core
    across = tp + 2 - 4 * lax.rem(z, 2)
    spot = lax.rem(z, 4)
    is_end = jnp.logical_or(spot == 0, spot == 3)
    is_inner = jnp.logical_not(is_end)
    upper = spot // 2
    inward = tp + 2 - 4 * upper
    outward = tp - 2 + 4 * upper
    tokens, model = toks.shape[1], toks.shape[2]
    top = route.shape[0]
    half = model // 2
    chunk = half // (2 * STEPS)
    base = core * half
    rows = n_ep * cap
    capp = cs.shape[2]
    units = wg.shape[1]
    width = out.shape[1]
    near = [d for d in range(1, n_ep) if not d & (d - 1)]
    far = [d for d in range(1, n_ep) if d & (d - 1)]
    everyone = [(peer_of(ep, d, n_ep), tp) for d in range(1, n_ep)]
    everyone += [(ep, lax.rem(tp + k, n_tp)) for k in range(1, n_tp)]

    def cols(start, size):
        return pl.ds(pl.multiple_of(start, LANES), size)

    loads = []
    for h in (core, 1 - core):
        for a, src in enumerate((tok_hbm, cot_hbm)):
            part = cols(h * half, half)
            loads.append(pltpu.make_async_copy(
                src.at[:, part], toks.at[a, :, part], local.at[len(loads)]
            ))
    for src, dst in ((wg_hbm, wg), (wu_hbm, wu), (wd_hbm, wd)):
        loads.append(pltpu.make_async_copy(src, dst, local.at[len(loads)]))
    for load in loads:
        load.start()
    entered = barrier(everyone)

    route_v = route[...]
    expert = lax.broadcasted_iota(jnp.int32, (-(-n_ep // 16) * 16, tokens), 0)
    names = jnp.zeros(expert.shape, F32)
    for k in range(top):
        names = names + jnp.where(route_v[k : k + 1] == expert, 1.0, 0.0)
    earlier = jnp.where(
        lax.broadcasted_iota(jnp.int32, (tokens, tokens), 0)
        < lax.broadcasted_iota(jnp.int32, (tokens, tokens), 1), 1.0, 0.0,
    ).astype(BF16)
    rank = jnp.dot(names.astype(BF16), earlier, preferred_element_type=F32)
    place_of = (expert * cap).astype(F32) + rank
    tab[...] = jnp.zeros_like(tab)
    slot_r = []
    for k in range(top):
        slot = jnp.sum(
            jnp.where(route_v[k : k + 1] == expert, place_of, 0.0), axis=0, keepdims=True
        )
        slot_r.append(slot)
        tab[k : k + 1, :] = slot
        tab[top + k : top + k + 1, :] = gates[...] * inner[k : k + 1, :]
    turned = tab[...].T
    slot_c = [turned[:, k : k + 1] for k in range(top)]
    comb_c = [turned[:, top + k : top + k + 1] for k in range(top)]

    def one_hot(index, slots):
        hit = index == slots[0]
        for slot in slots[1:]:
            hit = jnp.logical_or(hit, index == slot)
        return jnp.where(hit, 1.0, 0.0).astype(BF16)

    put[...] = one_hot(
        lax.broadcasted_iota(jnp.int32, (rows, tokens), 0).astype(F32), slot_r
    )
    own_put = one_hot(
        (lax.broadcasted_iota(jnp.int32, (cap, tokens), 0) + ep * cap).astype(F32), slot_r
    )

    def piece(a, p, k, side):
        return rows_v.at[a, p, :, cols(base + (k + STEPS * side) * chunk, chunk)]

    def direct(a, d, k, side, slot=0):
        p = peer_of(ep, d, n_ep)
        return remote(
            sends.at[a, p, :, cols((k + STEPS * side) * chunk, chunk)],
            piece(a, ep, k, side),
            drain.at[slot], recv.at[a, d - 1, k, side], p, tp,
        )

    def along(a, d, k, side, slot, target):
        p = peer_of(ep, d, n_ep)
        return remote(
            piece(a, p, k, side), piece(a, p, k, side),
            drain.at[slot], recv.at[a, d - 1, k, side], ep, target,
        )

    def to_sibling(a, d, k, side):
        p = peer_of(ep, d, n_ep)
        return remote(
            piece(a, p, k, side), piece(a, p, k, side),
            drain.at[4], sib_recv.at[a, d - 1, k, side], ep, sibling,
        )

    def place(k):
        for side in (1, 0):
            at = (k + STEPS * side) * chunk
            for a in range(2):
                placed = jnp.dot(
                    put[...], toks[a, :, cols(base + at, chunk)], preferred_element_type=F32
                ).astype(BF16).reshape(n_ep, cap, chunk)
                sends[a, :, :, cols(at, chunk)] = placed
                rows_v[a, ep, :, cols(base + at, chunk)] = sends[a, ep, :, cols(at, chunk)]

    def send_out(k):
        @pl.when(is_end)
        def _():
            for side in (1, 0):
                for a in range(2):
                    for d in near:
                        direct(a, d, k, side).start()

            @pl.when(k == STEPS - 1)
            def _():
                for a in range(2):
                    for d in far:
                        direct(a, d, k, 1 - upper, 1).start()

        @pl.when(is_inner)
        def _():
            for a in range(2):
                for d in far:
                    direct(a, d, k, upper).start()
            for a in range(2):
                for d in near:
                    direct(a, d, k, 0).start()

    loads[0].wait()
    loads[1].wait()
    place(0)
    entered()
    send_out(0)

    def place_step(k, carry):
        place(k)
        send_out(k)
        return carry

    lax.fori_loop(1, STEPS, place_step, 0)

    lane = lax.broadcasted_iota(jnp.int32, (tokens, capp), 1)
    lane_f = lane.astype(F32)
    for e in range(n_ep):
        weight = jnp.zeros((tokens, capp), F32)
        for k in range(top):
            hit = jnp.logical_and(lane_f == slot_c[k] - float(e * cap), lane < cap)
            weight = weight + jnp.where(hit, comb_c[k], 0.0)
        cs[e] = jnp.sum(weight, axis=0, keepdims=True)
    c_sends = []
    for d in range(1, n_ep):
        p = peer_of(ep, d, n_ep)
        copy = remote(cs.at[p], c_in.at[ep], c_s.at[d - 1], c_r.at[d - 1], p, tp)
        copy.start()
        c_sends.append(copy)
    c_in[ep] = cs[ep]
    pick[...] = one_hot(
        lax.broadcasted_iota(jnp.int32, (tokens, rows), 1).astype(F32), slot_c
    )
    square[...] = jnp.zeros_like(square)
    acc_g[...] = jnp.zeros_like(acc_g)
    acc_u[...] = jnp.zeros_like(acc_u)
    acc_h[...] = jnp.zeros_like(acc_h)
    loads[2].wait()
    loads[3].wait()
    other = (1 - core) * half
    for a in range(2):
        def own_step(j, carry, a=a):
            part = cols(other + j * (half // 4), half // 4)
            rows_v[a, ep, :, part] = jnp.dot(
                own_put, toks[a, :, part], preferred_element_type=F32
            ).astype(BF16)
            return carry

        lax.fori_loop(0, 4, own_step, 0)
    for load in loads[4:]:
        load.wait()

    def accumulate(h, k):
        parts = [cols(h * half + (k + STEPS * side) * chunk, chunk) for side in range(2)]

        def source(a, part):
            return rows_v[a, :, :, part].reshape(rows, chunk)

        for acc, w in ((acc_g, wg), (acc_u, wu)):
            acc[...] += jnp.dot(
                source(0, parts[0]), w[parts[0], :], preferred_element_type=F32
            ) + jnp.dot(source(0, parts[1]), w[parts[1], :], preferred_element_type=F32)
        acc_h[...] += dot_nt(source(1, parts[0]), wd[:, parts[0]]) + dot_nt(
            source(1, parts[1]), wd[:, parts[1]]
        )

    def arrive(k, carry):
        @pl.when(is_end)
        def _():
            for side in (1, 0):
                for a in range(2):
                    for d in near:
                        direct(a, d, k, side).wait_recv()
                        if side:
                            along(a, d, k, side, 2, inward).start()
                        to_sibling(a, d, k, side).start()
            for side in (upper, 1 - upper):
                for a in range(2):
                    for d in far:
                        direct(a, d, k, side).wait_recv()
                        to_sibling(a, d, k, side).start()

        @pl.when(is_inner)
        def _():
            for a in range(2):
                for d in far:
                    direct(a, d, k, upper).wait_recv()
                    along(a, d, k, upper, 2, inward).start()
                    along(a, d, k, upper, 3, outward).start()
                    to_sibling(a, d, k, upper).start()
            for a in range(2):
                for d in near:
                    direct(a, d, k, 0).wait_recv()
                    to_sibling(a, d, k, 0).start()
            for a in range(2):
                for d in far:
                    direct(a, d, k, 1 - upper).wait_recv()

                    @pl.when(k < STEPS - 1)
                    def _():
                        along(a, d, k, 1 - upper, 3, outward).start()

                    to_sibling(a, d, k, 1 - upper).start()
            for a in range(2):
                for d in near:
                    direct(a, d, k, 1).wait_recv()
                    to_sibling(a, d, k, 1).start()

        accumulate(core, k)
        for a in range(2):
            for side in range(2):
                for d in range(1, n_ep):
                    to_sibling(a, d, k, side).wait_recv()
        accumulate(1 - core, k)
        return carry

    lax.fori_loop(0, STEPS, arrive, 0)
    for copy in c_sends:
        copy.wait_recv()

    for p in range(n_ep):
        part = pl.ds(p * cap, cap)
        weight = jnp.broadcast_to(c_in[p], (LANES, capp)).T[:cap, :1]
        gate, up, grad = acc_g[part, :], acc_u[part, :], acc_h[part, :]
        sig = jax.nn.sigmoid(gate)
        silu = gate * sig
        hidden = silu * up
        score = jnp.sum(grad * hidden.astype(BF16).astype(F32), axis=1, keepdims=True)
        square[:cap, :] = jnp.broadcast_to(score, (cap, LANES))
        sc_in[tp, p] = square[...].T[:1, :]
        weighted = weight * grad
        hid[part, :] = (weight * hidden).astype(BF16)
        ggu[part, :units] = (weighted * up * sig * (1.0 + gate * (1.0 - sig))).astype(BF16)
        ggu[part, units:] = (weighted * silu).astype(BF16)

    def partial(share):
        part = pl.ds(pl.multiple_of(share * width, width), width)
        return dot_nt(ggu[:, :units], wg[part, :]) + dot_nt(ggu[:, units:], wu[part, :])

    masks = [1] + list(range(nz - 1, 1, -1)) + [0]
    order = [peer_of(z, m, nz) for m in masks]
    waits = []
    halves, moves = {}, {}

    def give_half(i):
        first[i] = partial(2 * order[i] + 1 - core).astype(BF16)
        halves[i] = remote(first.at[i], first_in.at[i], s1.at[i], r1.at[i], ep, sibling)
        halves[i].start()

    def spread(i):
        for d in range(1, n_ep):
            p = peer_of(ep, d, n_ep)
            copy = remote(
                second.at[i - 1, p], second_in.at[i - 1, ep],
                s2.at[i - 1, d - 1], r2.at[i - 1, d - 1], p, tp,
            )
            copy.start()
            moves[i, d] = copy

    crossing = remote(across_v, across_in, sa, ra, ep, across)

    def join(i):
        total = partial(2 * order[i] + core)
        halves[i].wait_recv()
        total = total + first_in[i].astype(F32)
        if i == 0:
            across_v[...] = total.astype(BF16)
            crossing.start()
        elif i < nz - 1:
            second[i - 1] = total.astype(BF16).reshape(second.shape[1:])
            spread(i)
        else:
            own_total[...] = total

    for i in range(nz):
        give_half(i)
        if i:
            join(i - 1)
    join(nz - 1)
    sc_sends = []
    for k in range(1, n_tp):
        copy = remote(
            sc_in.at[tp], sc_in.at[tp], sc_s.at[k - 1], sc_r.at[k - 1],
            ep, lax.rem(tp + k, n_tp),
        )
        copy.start()
        sc_sends.append(copy)

    def tile(t):
        return pl.ds(pl.multiple_of(t * width, width), width)

    def gate_up_step(t, carry):
        both = lax.dot_general(
            rows_v[0, :, :, tile(t)].reshape(rows, width), ggu[...],
            (((0,), (0,)), ((), ())), preferred_element_type=F32,
        ).astype(BF16)
        gate_out[tile(t), :] = both[:, :units]
        up_out[tile(t), :] = both[:, units:]
        return carry

    hidden_t = hid[...].T

    def down_step(t, carry):
        down_out[:, tile(t)] = jnp.dot(
            hidden_t, rows_v[1, :, :, tile(t)].reshape(rows, width),
            preferred_element_type=F32,
        ).astype(BF16)
        return carry

    def gather_tokens(i):
        for d in range(1, n_ep):
            moves[i, d].wait_recv()
        second_in[i - 1, ep] = second[i - 1, ep]
        return jnp.dot(
            pick[...], second_in[i - 1].reshape(rows, width), preferred_element_type=F32
        )

    last = []

    def pass_on(i):
        third[i - 1] = gather_tokens(i).astype(BF16)
        copy = remote(
            third.at[i - 1], third_in.at[i - 1], s3.at[i - 1], r3.at[i - 1],
            ep, 2 * order[i] + core,
        )
        copy.start()
        last.append(copy)

    lax.fori_loop(0, n_tp, gate_up_step, 0)
    pass_on(1)
    lax.fori_loop(0, n_tp // 2, down_step, 0)
    crossing.wait_recv()
    total = own_total[...] + across_in[...].astype(F32)
    second[nz - 2] = total.astype(BF16).reshape(second.shape[1:])
    spread(nz - 1)
    for i in range(2, nz - 1):
        pass_on(i)

    for copy in sc_sends:
        copy.wait_recv()
    summed = sc_in[0]
    for t in range(1, n_tp):
        summed = summed + sc_in[t]
    tot[...] = summed
    tot_sends = []
    for d in range(1, n_ep):
        p = peer_of(ep, d, n_ep)
        copy = remote(tot.at[p], tot_in.at[ep], tot_s.at[d - 1], tot_r.at[d - 1], p, tp)
        copy.start()
        tot_sends.append(copy)
    tot_in[ep] = tot[ep]
    lax.fori_loop(n_tp // 2, n_tp, down_step, 0)
    for copy in tot_sends:
        copy.wait_recv()
    score_r = [jnp.zeros((1, tokens), F32) for _ in range(top)]
    for e in range(n_ep):
        column = jnp.broadcast_to(tot_in[e], (LANES, capp)).T[:cap, :1]
        index = (lax.broadcasted_iota(jnp.int32, (cap, tokens), 0) + e * cap).astype(F32)
        for k in range(top):
            score_r[k] = score_r[k] + jnp.sum(
                jnp.where(index == tab[k : k + 1, :], column, 0.0), axis=0, keepdims=True
            )
    group = jnp.zeros((1, tokens), F32)
    for k in range(top):
        inner_out[k : k + 1, :] = gates[...] * score_r[k]
        group = group + inner[k : k + 1, :] * score_r[k]
    group_out[...] = group

    total = gather_tokens(nz - 1)
    for i, copy in enumerate(last):
        copy.wait_recv()
        total = total + third_in[i].astype(F32)
    out[...] = total.astype(BF16)

    def drained(ref, slot):
        remote(ref, ref, drain.at[slot], drain.at[slot], ep, sibling).wait_send()

    @pl.when(is_end)
    def _():
        drained(sends.at[:, : len(near)], 0)
        if far:
            drained(sends.at[:, : len(far), :, :chunk], 1)
        drained(rows_v.at[:, : len(near), :, : half // 2], 2)

    @pl.when(is_inner)
    def _():
        drained(sends.at[:, : n_ep - 1, :, : half // 2], 0)
        if far:
            drained(rows_v.at[:, : len(far), :, : half // 2], 2)
            drained(rows_v.at[:, : len(far), :, : half - chunk], 3)

    drained(rows_v.at[:, : n_ep - 1, :, :half], 4)
    for copy in c_sends + sc_sends + tot_sends + list(halves.values()) + list(moves.values()) + last:
        copy.wait_send()
    crossing.wait_send()


def layer(n_ep, n_tp, cap, route, gates, inner, tokens, cotangent, wg, wu, wd):
    vmem = pl.BlockSpec(memory_space=pltpu.VMEM)
    any_spec = pl.BlockSpec(memory_space=pl.ANY)
    nz = n_tp // 2
    count, model = tokens.shape
    rows, units = n_ep * cap, wg.shape[1]
    width, half = model // n_tp, model // 2
    capp = -(-cap // LANES) * LANES
    dma = pltpu.SemaphoreType.DMA
    return pl.pallas_call(
        functools.partial(layer_kernel, n_ep, n_tp, cap),
        out_shape=(
            jax.ShapeDtypeStruct((count, width), BF16),
            jax.ShapeDtypeStruct(gates.shape, F32),
            jax.ShapeDtypeStruct(inner.shape, F32),
            jax.ShapeDtypeStruct(wg.shape, BF16),
            jax.ShapeDtypeStruct(wu.shape, BF16),
            jax.ShapeDtypeStruct(wd.shape, BF16),
        ),
        in_specs=[vmem] * 3 + [any_spec] * 5,
        out_specs=(vmem,) * 6,
        scratch_shapes=[
            pltpu.VMEM((2, count, model), BF16),
            pltpu.VMEM((2, n_ep, cap, half), BF16),
            pltpu.VMEM((2, n_ep, cap, model), BF16),
            pltpu.VMEM(wg.shape, BF16),
            pltpu.VMEM(wu.shape, BF16),
            pltpu.VMEM(wd.shape, BF16),
            pltpu.VMEM((8, count), F32),
            pltpu.VMEM((rows, count), BF16),
            pltpu.VMEM((count, rows), BF16),
            pltpu.VMEM((n_ep, 1, capp), F32),
            pltpu.VMEM((n_ep, 1, capp), F32),
            pltpu.VMEM((capp, LANES), F32),
            pltpu.VMEM((n_tp, n_ep, 1, capp), F32),
            pltpu.VMEM((n_ep, 1, capp), F32),
            pltpu.VMEM((n_ep, 1, capp), F32),
            pltpu.VMEM((rows, units), F32),
            pltpu.VMEM((rows, units), F32),
            pltpu.VMEM((rows, units), F32),
            pltpu.VMEM((rows, 2 * units), BF16),
            pltpu.VMEM((rows, units), BF16),
            pltpu.VMEM((nz, rows, width), BF16),
            pltpu.VMEM((nz, rows, width), BF16),
            pltpu.VMEM((nz - 1, n_ep, cap, width), BF16),
            pltpu.VMEM((nz - 1, n_ep, cap, width), BF16),
            pltpu.VMEM((rows, width), BF16),
            pltpu.VMEM((rows, width), BF16),
            pltpu.VMEM((rows, width), F32),
            pltpu.VMEM((nz - 2, count, width), BF16),
            pltpu.VMEM((nz - 2, count, width), BF16),
            dma((7,)),
            dma((5,)),
            dma((2, n_ep - 1, STEPS, 2)),
            dma((2, n_ep - 1, STEPS, 2)),
            dma((n_ep - 1,)), dma((n_ep - 1,)),
            dma((n_tp - 1,)), dma((n_tp - 1,)),
            dma((n_ep - 1,)), dma((n_ep - 1,)),
            dma((nz,)), dma((nz,)),
            dma((nz - 1, n_ep - 1)), dma((nz - 1, n_ep - 1)),
            dma((nz - 2,)), dma((nz - 2,)),
            dma, dma,
        ],
        compiler_params=pltpu.CompilerParams(
            collective_id=0, has_side_effects=True, vmem_limit_bytes=54 * 1024 * 1024
        ),
    )(route, gates, inner, tokens, cotangent, wg, wu, wd)


def deliver_kernel(count, *refs):
    sems = refs[-1]
    copies = [
        pltpu.make_async_copy(refs[i], refs[count + i], sems.at[i]) for i in range(count)
    ]
    for copy in copies:
        copy.start()
    for copy in copies:
        copy.wait()


def deliver(*arrays):
    count = len(arrays)
    return pl.pallas_call(
        functools.partial(deliver_kernel, count),
        out_shape=tuple(jax.ShapeDtypeStruct(a.shape, a.dtype) for a in arrays),
        in_specs=[pl.BlockSpec(memory_space=pltpu.VMEM)] * count,
        out_specs=(pl.BlockSpec(memory_space=pl.ANY),) * count,
        scratch_shapes=[pltpu.SemaphoreType.DMA((count,))],
    )(*arrays)


def per_device(tokens, cotangent, routing, group_gate, inner_gate, w_gate, w_up, w_down):
    n_ep, n_tp = lax.axis_size("ep"), lax.axis_size("tp")
    cap = tokens.shape[0] * routing.shape[1] * 5 // (4 * n_ep)
    results = layer(
        n_ep, n_tp, cap, routing.T, group_gate[None], inner_gate.T,
        tokens, cotangent, w_gate[0], w_up[0], w_down[0],
    )
    token_grad, group_grad, inner_grad, gate_grad, upper_grad, down_grad = deliver(*results)
    return (
        token_grad,
        group_grad[0],
        inner_grad.T,
        gate_grad[None],
        upper_grad[None],
        down_grad[None],
    )


def solution(mesh):
    return jax.shard_map(
        per_device,
        mesh=mesh,
        in_specs=(
            P("ep", None),
            P("ep", None),
            P("ep", None),
            P("ep"),
            P("ep", None),
            P("ep", None, "tp"),
            P("ep", None, "tp"),
            P("ep", "tp", None),
        ),
        out_specs=(
            P("ep", "tp"),
            P("ep"),
            P("ep", None),
            P("ep", None, "tp"),
            P("ep", None, "tp"),
            P("ep", "tp", None),
        ),
        check_vma=False,
    )
```

time: 132 us -> 105 us (0.80)
  matrix products: 20.7 us -> 0 us
  Pallas kernels: 92.1 us -> 104 us
  local copies, waits for them, and re-layouts: 11.8 us -> 0 us
  other arithmetic: 5.85 us -> 0 us
    dot_general x6 -> x0, matrix products: 20.7 us -> none  [the longest x2 7.68 us: placed(): jnp.dot(put, source, preferred_element_type=F32).astype(BF16)]
    pallas_call x2, Pallas kernels: 92.1 us -> 104 us  [the longest x1 98.3 us: layer(): pl.pallas_call(functools.partial(layer_kernel, n_ep, n_tp, cap), out_shap...]
    unnamed x22 -> x0, local copies, waits for them, and re-layouts: 9.03 us -> none
    reduce_sum x5 -> x0, other arithmetic: 2.84 us -> none  [the longest x1 0.85 us: per_device(): jnp.sum((route_t[:, None, :] == experts[None, :, None]).astype(F32), axis=0)]
where the time goes in v1:
time: 105 us
  Pallas kernels  104 us (99%)
    pallas_call x1, Pallas kernels, layer(): pl.pallas_call(functools.partial(layer_kernel, n_ep, n_tp, cap), out_shap...  98.3 us
    pallas_call x1, Pallas kernels, deliver(): pl.pallas_call(functools.partial(deliver_kernel, count), out_shape=tuple(...  5.8 us

profile of v1, /device:TPU:0, one launch (start us, length us, event | category | flops | bytes accessed | tf_op | source)
XLA Modules:
  0.0 104.7 jit_solution(11980808769787036332)
XLA Ops:
  0.6 98.3 %shard_map.127 = (bf16[256,512]{1,0:T(8,128)(2,1)}, f32[1,256]{1,0:T(1,128)}, f32[2,256]{1,0:T(2,128)}, bf16[4096,256]{1,0:T(8,128)(2,1)}, bf16[4096,256]{1,0:T(8,128)(2,1)}, /*index=5*/bf16[256,4096]{1,0:T(8,128)(2,1)}) custom-call(s32[2,256]{1,0:T(2,128)} %bitcast.14, f32[1,256]{1,0:T(1,128)} %bitcast.16, f32[2,256]{1,0:T(2,128)} %bitcast.15, ...), custom_call_target="tpu_custom_call" | custom-call | tf_op jit(solution)/shard_map/pallas_call | solution.py:500
  98.9 5.8 %shard_map.128 = (bf16[256,512]{1,0:T(8,128)(2,1)}, f32[1,256]{1,0:T(1,128)}, f32[2,256]{1,0:T(2,128)}, bf16[4096,256]{1,0:T(8,128)(2,1)}, bf16[4096,256]{1,0:T(8,128)(2,1)}, /*index=5*/bf16[256,4096]{1,0:T(8,128)(2,1)}) custom-call(bf16[256,512]{1,0:T(8,128)(2,1)} %get-tuple-element.18.refs_0_, f32[1,256]{1,0:T(1,128)} %get-tuple-element.19.refs_1_, ...), custom_call_target="tpu_custom_call" | custom-call | tf_op jit(solution)/shard_map/pallas_call | solution.py:573

commit v2 on v1

--- a/solution.py
+++ b/solution.py
@@ -53,9 +53,10 @@
                  toks, sends, rows_v, wg, wu, wd, tab, put, pick,
                  cs, c_in, square, sc_in, tot, tot_in,
                  acc_g, acc_u, acc_h, ggu, hid,
-                 first, first_in, second, second_in, across_v, across_in, own_total, third, third_in,
+                 first, first_in, second, second_in, across_v, across_in, own_total,
+                 third, third_in, held, final_in,
                  local, drain, recv, sib_recv, c_s, c_r, sc_s, sc_r, tot_s, tot_r,
-                 s1, r1, s2, r2, s3, r3, sa, ra):
+                 s1, r1, s2, r2, s3, r3, s4, r4, sa, ra):
     ep, tp = lax.axis_index("ep"), lax.axis_index("tp")
     core = lax.rem(tp, 2)
     z = tp // 2
@@ -192,6 +193,12 @@
             for a in range(2):
                 for d in near:
                     direct(a, d, k, 0).start()
+
+            @pl.when(k == STEPS - 1)
+            def _():
+                for a in range(2):
+                    for d in near:
+                        direct(a, d, k, 1, 1).start()
 
     loads[0].wait()
     loads[1].wait()
@@ -257,57 +264,76 @@
             source(1, parts[1]), wd[:, parts[1]]
         )
 
-    def arrive(k, carry):
-        @pl.when(is_end)
-        def _():
-            for side in (1, 0):
-                for a in range(2):
-                    for d in near:
-                        direct(a, d, k, side).wait_recv()
-                        if side:
-                            along(a, d, k, side, 2, inward).start()
-                        to_sibling(a, d, k, side).start()
-            for side in (upper, 1 - upper):
-                for a in range(2):
-                    for d in far:
-                        direct(a, d, k, side).wait_recv()
-                        to_sibling(a, d, k, side).start()
-
-        @pl.when(is_inner)
-        def _():
-            for a in range(2):
-                for d in far:
-                    direct(a, d, k, upper).wait_recv()
-                    along(a, d, k, upper, 2, inward).start()
-                    along(a, d, k, upper, 3, outward).start()
-                    to_sibling(a, d, k, upper).start()
-            for a in range(2):
-                for d in near:
-                    direct(a, d, k, 0).wait_recv()
-                    to_sibling(a, d, k, 0).start()
-            for a in range(2):
-                for d in far:
-                    direct(a, d, k, 1 - upper).wait_recv()
-
-                    @pl.when(k < STEPS - 1)
-                    def _():
-                        along(a, d, k, 1 - upper, 3, outward).start()
-
-                    to_sibling(a, d, k, 1 - upper).start()
-            for a in range(2):
-                for d in near:
-                    direct(a, d, k, 1).wait_recv()
-                    to_sibling(a, d, k, 1).start()
-
+    def taken(ds, k, side, *targets):
+        for a in range(2):
+            for d in ds:
+                direct(a, d, k, side).wait_recv()
+                for slot, target in targets:
+                    along(a, d, k, side, slot, target).start()
+                to_sibling(a, d, k, side).start()
+
+    def finish(k):
         accumulate(core, k)
         for a in range(2):
             for side in range(2):
                 for d in range(1, n_ep):
                     to_sibling(a, d, k, side).wait_recv()
         accumulate(1 - core, k)
+
+    def arrive(k, carry):
+        @pl.when(jnp.logical_and(is_end, k < STEPS - 1))
+        def _():
+            taken(near, k, 1, (2, inward))
+
+        @pl.when(jnp.logical_and(is_end, k == STEPS - 1))
+        def _():
+            taken(near, k, 1)
+
+        @pl.when(is_end)
+        def _():
+            @pl.when(k > 0)
+            def _():
+                taken(far, k - 1, upper)
+
+            taken(near, k, 0)
+
+            @pl.when(k > 0)
+            def _():
+                taken(far, k - 1, 1 - upper)
+
+        @pl.when(is_inner)
+        def _():
+            taken(far, k, upper, (2, inward), (3, outward))
+
+            @pl.when(k > 0)
+            def _():
+                taken(near, k - 1, 1)
+
+            taken(near, k, 0)
+
+        @pl.when(jnp.logical_and(is_inner, k < STEPS - 1))
+        def _():
+            taken(far, k, 1 - upper, (3, outward))
+
+        @pl.when(jnp.logical_and(is_inner, k == STEPS - 1))
+        def _():
+            taken(near, k, 1)
+            taken(far, k, 1 - upper)
+
+        @pl.when(k > 0)
+        def _():
+            finish(k - 1)
+
         return carry
 
     lax.fori_loop(0, STEPS, arrive, 0)
+
+    @pl.when(is_end)
+    def _():
+        taken(far, STEPS - 1, upper)
+        taken(far, STEPS - 1, 1 - upper)
+
+    finish(STEPS - 1)
     for copy in c_sends:
         copy.wait_recv()
 
@@ -330,9 +356,26 @@
         part = pl.ds(pl.multiple_of(share * width, width), width)
         return dot_nt(ggu[:, :units], wg[part, :]) + dot_nt(ggu[:, units:], wu[part, :])
 
-    masks = [1] + list(range(nz - 1, 1, -1)) + [0]
-    order = [peer_of(z, m, nz) for m in masks]
-    waits = []
+    sc_sends = []
+    for k in range(1, n_tp):
+        copy = remote(
+            sc_in.at[tp], sc_in.at[tp], sc_s.at[k - 1], sc_r.at[k - 1],
+            ep, lax.rem(tp + k, n_tp),
+        )
+        copy.start()
+        sc_sends.append(copy)
+
+    pairs, pair = nz // 2, z // 2
+    owners = []
+    for m in range(1, pairs):
+        them = peer_of(pair, m, pairs)
+        odd = lax.rem(them, 2)
+        owners += [(m, 2 * them + odd), (m, 2 * them + 1 - odd)]
+    n_far = 2 * len(owners)
+    side, own = n_far, n_far + 1
+    order = [q for _, q in owners[:1]] + [2 * pair + 1 - lax.rem(z, 2)]
+    order += [q for _, q in owners[1:]] + [z]
+    split = width // 2
     halves, moves = {}, {}
 
     def give_half(i):
@@ -340,15 +383,14 @@
         halves[i] = remote(first.at[i], first_in.at[i], s1.at[i], r1.at[i], ep, sibling)
         halves[i].start()
 
-    def spread(i):
+    def spread(n):
         for d in range(1, n_ep):
             p = peer_of(ep, d, n_ep)
             copy = remote(
-                second.at[i - 1, p], second_in.at[i - 1, ep],
-                s2.at[i - 1, d - 1], r2.at[i - 1, d - 1], p, tp,
+                second.at[n, p], second_in.at[n, ep], s2.at[n, d - 1], r2.at[n, d - 1], p, tp
             )
             copy.start()
-            moves[i, d] = copy
+            moves[n, d] = copy
 
     crossing = remote(across_v, across_in, sa, ra, ep, across)
 
@@ -356,28 +398,28 @@
         total = partial(2 * order[i] + core)
         halves[i].wait_recv()
         total = total + first_in[i].astype(F32)
-        if i == 0:
-            across_v[...] = total.astype(BF16)
+        low, high = total[:, :split], total[:, split:].astype(BF16).reshape(second.shape[1:])
+        if i == 1:
+            across_v[...] = low.astype(BF16)
             crossing.start()
+            second[side] = high
         elif i < nz - 1:
-            second[i - 1] = total.astype(BF16).reshape(second.shape[1:])
-            spread(i)
+            n = 2 * max(i - 1, 0)
+            second[n] = low.astype(BF16).reshape(second.shape[1:])
+            spread(n)
+            second[n + 1] = high
+            spread(n + 1)
         else:
-            own_total[...] = total
+            own_total[...] = low
+            second[own + 1] = high
+            spread(side)
+            spread(own + 1)
 
     for i in range(nz):
         give_half(i)
         if i:
             join(i - 1)
     join(nz - 1)
-    sc_sends = []
-    for k in range(1, n_tp):
-        copy = remote(
-            sc_in.at[tp], sc_in.at[tp], sc_s.at[k - 1], sc_r.at[k - 1],
-            ep, lax.rem(tp + k, n_tp),
-        )
-        copy.start()
-        sc_sends.append(copy)
 
     def tile(t):
         return pl.ds(pl.multiple_of(t * width, width), width)
@@ -400,49 +442,87 @@
         ).astype(BF16)
         return carry
 
-    def gather_tokens(i):
+    def gather_tokens(n):
         for d in range(1, n_ep):
-            moves[i, d].wait_recv()
-        second_in[i - 1, ep] = second[i - 1, ep]
+            moves[n, d].wait_recv()
+        second_in[n, ep] = second[n, ep]
         return jnp.dot(
-            pick[...], second_in[i - 1].reshape(rows, width), preferred_element_type=F32
-        )
-
-    last = []
-
-    def pass_on(i):
-        third[i - 1] = gather_tokens(i).astype(BF16)
-        copy = remote(
-            third.at[i - 1], third_in.at[i - 1], s3.at[i - 1], r3.at[i - 1],
-            ep, 2 * order[i] + core,
-        )
-        copy.start()
-        last.append(copy)
-
-    lax.fori_loop(0, n_tp, gate_up_step, 0)
-    pass_on(1)
-    lax.fori_loop(0, n_tp // 2, down_step, 0)
-    crossing.wait_recv()
-    total = own_total[...] + across_in[...].astype(F32)
-    second[nz - 2] = total.astype(BF16).reshape(second.shape[1:])
-    spread(nz - 1)
-    for i in range(2, nz - 1):
-        pass_on(i)
-
-    for copy in sc_sends:
-        copy.wait_recv()
-    summed = sc_in[0]
-    for t in range(1, n_tp):
-        summed = summed + sc_in[t]
-    tot[...] = summed
+            pick[...], second_in[n].reshape(rows, split), preferred_element_type=F32
+        )
+
+    def to_collector(n):
+        return remote(third.at[n], third_in.at[n], s3.at[n], r3.at[n], ep, across)
+
+    def to_owner(n):
+        m, q = owners[n // 2]
+        slot = 2 * (m - 1) + n % 2
+        return remote(
+            third.at[n], final_in.at[slot], s4.at[n], r4.at[slot], ep, 2 * q + core
+        )
+
+    def gather_far(n):
+        summed = gather_tokens(n)
+
+        @pl.when(is_end)
+        def _():
+            third[n] = summed.astype(BF16)
+            to_collector(n).start()
+
+        @pl.when(is_inner)
+        def _():
+            held[n] = summed
+
+    def collect(n):
+        @pl.when(is_inner)
+        def _():
+            to_collector(n).wait_recv()
+            third[n] = (held[n] + third_in[n].astype(F32)).astype(BF16)
+            to_owner(n).start()
+
+    def gate_up(part):
+        lax.fori_loop(part * n_tp // 2, (part + 1) * n_tp // 2, gate_up_step, 0)
+
+    def share_scores():
+        for copy in sc_sends:
+            copy.wait_recv()
+        summed = sc_in[0]
+        for t in range(1, n_tp):
+            summed = summed + sc_in[t]
+        tot[...] = summed
+        for d in range(1, n_ep):
+            p = peer_of(ep, d, n_ep)
+            copy = remote(tot.at[p], tot_in.at[ep], tot_s.at[d - 1], tot_r.at[d - 1], p, tp)
+            copy.start()
+            tot_sends.append(copy)
+        tot_in[ep] = tot[ep]
+
+    def cross():
+        crossing.wait_recv()
+        total = own_total[...] + across_in[...].astype(F32)
+        second[own] = total.astype(BF16).reshape(second.shape[1:])
+        spread(own)
+
+    def down(part):
+        lax.fori_loop(part * n_tp // 2, (part + 1) * n_tp // 2, down_step, 0)
+
     tot_sends = []
-    for d in range(1, n_ep):
-        p = peer_of(ep, d, n_ep)
-        copy = remote(tot.at[p], tot_in.at[ep], tot_s.at[d - 1], tot_r.at[d - 1], p, tp)
-        copy.start()
-        tot_sends.append(copy)
-    tot_in[ep] = tot[ep]
-    lax.fori_loop(n_tp // 2, n_tp, down_step, 0)
+    work = [
+        lambda: gate_up(0), lambda: gate_up(1), share_scores, cross,
+        lambda: down(0), lambda: down(1),
+    ]
+    for n in range(n_far):
+        gather_far(n)
+        for job in work[2 * n : 2 * n + 2]:
+            job()
+        if n:
+            collect(n - 1)
+    side_copy = remote(
+        third.at[side], final_in.at[2 * (pairs - 1)],
+        s4.at[side], r4.at[2 * (pairs - 1)], ep, across,
+    )
+    third[side] = gather_tokens(side).astype(BF16)
+    side_copy.start()
+    collect(n_far - 1)
     for copy in tot_sends:
         copy.wait_recv()
     score_r = [jnp.zeros((1, tokens), F32) for _ in range(top)]
@@ -459,11 +539,21 @@
         group = group + inner[k : k + 1, :] * score_r[k]
     group_out[...] = group
 
-    total = gather_tokens(nz - 1)
-    for i, copy in enumerate(last):
-        copy.wait_recv()
-        total = total + third_in[i].astype(F32)
-    out[...] = total.astype(BF16)
+    def final_copy(slot):
+        return remote(
+            third.at[0], final_in.at[slot], s4.at[0], r4.at[slot], ep, across
+        )
+
+    high, low = gather_tokens(own + 1), gather_tokens(own)
+    side_copy.wait_recv()
+    high = high + final_in[2 * (pairs - 1)].astype(F32)
+    for m in range(pairs - 1):
+        final_copy(2 * m).wait_recv()
+        low = low + final_in[2 * m].astype(F32)
+        final_copy(2 * m + 1).wait_recv()
+        high = high + final_in[2 * m + 1].astype(F32)
+    out[:, :split] = low.astype(BF16)
+    out[:, split:] = high.astype(BF16)
 
     def drained(ref, slot):
         remote(ref, ref, drain.at[slot], drain.at[slot], ep, sibling).wait_send()
@@ -473,19 +563,31 @@
         drained(sends.at[:, : len(near)], 0)
         if far:
             drained(sends.at[:, : len(far), :, :chunk], 1)
-        drained(rows_v.at[:, : len(near), :, : half // 2], 2)
+        drained(rows_v.at[:, : len(near), :, : half // 2 - chunk], 2)
 
     @pl.when(is_inner)
     def _():
         drained(sends.at[:, : n_ep - 1, :, : half // 2], 0)
+        drained(sends.at[:, : len(near), :, :chunk], 1)
         if far:
             drained(rows_v.at[:, : len(far), :, : half // 2], 2)
             drained(rows_v.at[:, : len(far), :, : half - chunk], 3)
 
     drained(rows_v.at[:, : n_ep - 1, :, :half], 4)
-    for copy in c_sends + sc_sends + tot_sends + list(halves.values()) + list(moves.values()) + last:
+    for copy in c_sends + sc_sends + tot_sends + list(halves.values()) + list(moves.values()):
         copy.wait_send()
     crossing.wait_send()
+    side_copy.wait_send()
+
+    @pl.when(is_end)
+    def _():
+        for n in range(n_far):
+            to_collector(n).wait_send()
+
+    @pl.when(is_inner)
+    def _():
+        for n in range(n_far):
+            to_owner(n).wait_send()
 
 
 def layer(n_ep, n_tp, cap, route, gates, inner, tokens, cotangent, wg, wu, wd):
@@ -500,12 +602,12 @@
     return pl.pallas_call(
         functools.partial(layer_kernel, n_ep, n_tp, cap),
         out_shape=(
-            jax.ShapeDtypeStruct((count, width), BF16),
-            jax.ShapeDtypeStruct(gates.shape, F32),
-            jax.ShapeDtypeStruct(inner.shape, F32),
-            jax.ShapeDtypeStruct(wg.shape, BF16),
-            jax.ShapeDtypeStruct(wu.shape, BF16),
-            jax.ShapeDtypeStruct(wd.shape, BF16),
+            pltpu.VMEM((count, width), BF16),
+            pltpu.VMEM(gates.shape, F32),
+            pltpu.VMEM(inner.shape, F32),
+            pltpu.VMEM(wg.shape, BF16),
+            pltpu.VMEM(wu.shape, BF16),
+            pltpu.VMEM(wd.shape, BF16),
         ),
         in_specs=[vmem] * 3 + [any_spec] * 5,
         out_specs=(vmem,) * 6,
@@ -532,13 +634,15 @@
             pltpu.VMEM((rows, units), BF16),
             pltpu.VMEM((nz, rows, width), BF16),
             pltpu.VMEM((nz, rows, width), BF16),
-            pltpu.VMEM((nz - 1, n_ep, cap, width), BF16),
-            pltpu.VMEM((nz - 1, n_ep, cap, width), BF16),
-            pltpu.VMEM((rows, width), BF16),
-            pltpu.VMEM((rows, width), BF16),
-            pltpu.VMEM((rows, width), F32),
-            pltpu.VMEM((nz - 2, count, width), BF16),
-            pltpu.VMEM((nz - 2, count, width), BF16),
+            pltpu.VMEM((2 * nz - 1, n_ep, cap, width // 2), BF16),
+            pltpu.VMEM((2 * nz - 1, n_ep, cap, width // 2), BF16),
+            pltpu.VMEM((rows, width // 2), BF16),
+            pltpu.VMEM((rows, width // 2), BF16),
+            pltpu.VMEM((rows, width // 2), F32),
+            pltpu.VMEM((2 * nz - 3, count, width // 2), BF16),
+            pltpu.VMEM((2 * nz - 4, count, width // 2), BF16),
+            pltpu.VMEM((2 * nz - 4, count, width // 2), F32),
+            pltpu.VMEM((nz - 1, count, width // 2), BF16),
             dma((7,)),
             dma((5,)),
             dma((2, n_ep - 1, STEPS, 2)),
@@ -547,8 +651,9 @@
             dma((n_tp - 1,)), dma((n_tp - 1,)),
             dma((n_ep - 1,)), dma((n_ep - 1,)),
             dma((nz,)), dma((nz,)),
-            dma((nz - 1, n_ep - 1)), dma((nz - 1, n_ep - 1)),
-            dma((nz - 2,)), dma((nz - 2,)),
+            dma((2 * nz - 1, n_ep - 1)), dma((2 * nz - 1, n_ep - 1)),
+            dma((2 * nz - 4,)), dma((2 * nz - 4,)),
+            dma((2 * nz - 3,)), dma((nz - 1,)),
             dma, dma,
         ],
         compiler_params=pltpu.CompilerParams(
@@ -576,6 +681,7 @@
         in_specs=[pl.BlockSpec(memory_space=pltpu.VMEM)] * count,
         out_specs=(pl.BlockSpec(memory_space=pl.ANY),) * count,
         scratch_shapes=[pltpu.SemaphoreType.DMA((count,))],
+        compiler_params=pltpu.CompilerParams(vmem_limit_bytes=4 * 1024 * 1024),
     )(*arrays)
 
 
@@ -586,7 +692,9 @@
         n_ep, n_tp, cap, routing.T, group_gate[None], inner_gate.T,
         tokens, cotangent, w_gate[0], w_up[0], w_down[0],
     )
-    token_grad, group_grad, inner_grad, gate_grad, upper_grad, down_grad = deliver(*results)
+    token_grad, group_grad, inner_grad, gate_grad, upper_grad, down_grad = deliver(*[
+        pltpu.with_memory_space_constraint(r, pltpu.VMEM) for r in results
+    ])
     return (
         token_grad,
         group_grad[0],

time: 105 us -> 78.6 us (0.75)
  Pallas kernels: 104 us -> 77.8 us
    pallas_call x1, Pallas kernels: 98.3 us -> 74.9 us  [layer(): pl.pallas_call(functools.partial(layer_kernel, n_ep, n_tp, cap), out_shap...]
    pallas_call x1, Pallas kernels: 5.8 us -> 2.85 us  [deliver(): pl.pallas_call(functools.partial(deliver_kernel, count), out_shape=tuple(...]
where the time goes in v2:
time: 78.6 us; the launch traced here: 78.4 us
  Pallas kernels  77.8 us (99%)
    pallas_call x1, Pallas kernels, layer(): pl.pallas_call(functools.partial(layer_kernel, n_ep, n_tp, cap), out_shap...  74.9 us
    pallas_call x1, Pallas kernels, deliver(): pl.pallas_call(functools.partial(deliver_kernel, count), out_shape=tuple(...  2.85 us

profile of v2, /device:TPU:0, one launch (start us, length us, event | category | flops | bytes accessed | tf_op | source)
XLA Modules:
  0.0 78.4 jit_solution(12411112217173570159)
XLA Ops:
  0.6 74.9 %shard_map.127 = (bf16[256,512]{1,0:T(8,128)(2,1)S(1)}, f32[1,256]{1,0:T(1,128)S(1)}, f32[2,256]{1,0:T(2,128)S(1)}, bf16[4096,256]{1,0:T(8,128)(2,1)S(1)}, bf16[...) custom-call(s32[2,256]{1,0:T(2,128)} %bitcast.14, f32[1,256]{1,0:T(1,128)} %bitcast.16, f32[2,256]{1,0:T(2,128)} %bitcast.15, ...), custom_call_target="tpu_custom_call" | custom-call | tf_op jit(solution)/shard_map/pallas_call | solution.py:602
  75.5 2.8 %shard_map.128 = (bf16[256,512]{1,0:T(8,128)(2,1)}, f32[1,256]{1,0:T(1,128)}, f32[2,256]{1,0:T(2,128)}, bf16[4096,256]{1,0:T(8,128)(2,1)}, bf16[4096,256]{1,0:T(8,128)(2,1)}, /*index=5*/bf16[256,4096]{1,0:T(8,128)(2,1)}) custom-call(bf16[256,512]{1,0:T(8,128)(2,1)S(1)} %get-tuple-element.18.refs_0_, f32[1,256]{1,0:T(1,128)S(1)} %get-tuple-element.19.refs_1_, ...), custom_call_target="tpu_custom_call" | custom-call | tf_op jit(solution)/shard_map/pallas_call | solution.py:678

commit v3 on v2

--- a/solution.py
+++ b/solution.py
@@ -174,31 +174,38 @@
     def send_out(k):
         @pl.when(is_end)
         def _():
-            for side in (1, 0):
-                for a in range(2):
-                    for d in near:
-                        direct(a, d, k, side).start()
+            for a in range(2):
+                for d in near:
+                    direct(a, d, k, 1).start()
 
             @pl.when(k == STEPS - 1)
             def _():
-                for a in range(2):
-                    for d in far:
-                        direct(a, d, k, 1 - upper, 1).start()
+                for d in far:
+                    direct(0, d, k, 1 - upper, 1).start()
+
+            for a in range(2):
+                for d in near:
+                    direct(a, d, k, 0).start()
 
         @pl.when(is_inner)
         def _():
             for a in range(2):
                 for d in far:
                     direct(a, d, k, upper).start()
-            for a in range(2):
-                for d in near:
-                    direct(a, d, k, 0).start()
+
+            @pl.when(k > 0)
+            def _():
+                for a in range(2):
+                    for d in near:
+                        direct(a, d, k - 1, 0).start()
 
             @pl.when(k == STEPS - 1)
             def _():
                 for a in range(2):
                     for d in near:
-                        direct(a, d, k, 1, 1).start()
+                        direct(a, d, k, 0).start()
+                for d in near:
+                    direct(0, d, k, 1, 1).start()
 
     loads[0].wait()
     loads[1].wait()
@@ -250,90 +257,114 @@
     for load in loads[4:]:
         load.wait()
 
-    def accumulate(h, k):
-        parts = [cols(h * half + (k + STEPS * side) * chunk, chunk) for side in range(2)]
-
-        def source(a, part):
-            return rows_v[a, :, :, part].reshape(rows, chunk)
-
+    def accumulate(h, k, side):
+        part = cols(h * half + (k + STEPS * side) * chunk, chunk)
+        source = [rows_v[a, :, :, part].reshape(rows, chunk) for a in range(2)]
         for acc, w in ((acc_g, wg), (acc_u, wu)):
-            acc[...] += jnp.dot(
-                source(0, parts[0]), w[parts[0], :], preferred_element_type=F32
-            ) + jnp.dot(source(0, parts[1]), w[parts[1], :], preferred_element_type=F32)
-        acc_h[...] += dot_nt(source(1, parts[0]), wd[:, parts[0]]) + dot_nt(
-            source(1, parts[1]), wd[:, parts[1]]
-        )
-
-    def taken(ds, k, side, *targets):
-        for a in range(2):
+            acc[...] += jnp.dot(source[0], w[part, :], preferred_element_type=F32)
+        acc_h[...] += dot_nt(source[1], wd[:, part])
+
+    def taken(ds, k, side, *targets, arrays=(0, 1)):
+        for a in arrays:
             for d in ds:
                 direct(a, d, k, side).wait_recv()
                 for slot, target in targets:
                     along(a, d, k, side, slot, target).start()
                 to_sibling(a, d, k, side).start()
 
-    def finish(k):
-        accumulate(core, k)
-        for a in range(2):
-            for side in range(2):
+    def finish(*pieces):
+        for k, side in pieces:
+            accumulate(core, k, side)
+        return pieces
+
+    def finish_other(pieces):
+        for k, side in pieces:
+            for a in range(2):
                 for d in range(1, n_ep):
                     to_sibling(a, d, k, side).wait_recv()
-        accumulate(1 - core, k)
-
-    def arrive(k, carry):
-        @pl.when(jnp.logical_and(is_end, k < STEPS - 1))
+            accumulate(1 - core, k, side)
+
+    def arrive_end(k, carry):
+        @pl.when(k < STEPS - 1)
         def _():
             taken(near, k, 1, (2, inward))
 
-        @pl.when(jnp.logical_and(is_end, k == STEPS - 1))
-        def _():
+        @pl.when(k == STEPS - 1)
+        def _():
+            taken(near, k, 1, (2, inward), arrays=(1,))
+            taken(near, k, 1, arrays=(0,))
+
+        @pl.when(k > 0)
+        def _():
+            taken(far, k - 1, 1 - upper)
+
+        taken(far, k, upper)
+
+        @pl.when(k > 0)
+        def _():
+            finish((k - 1, 1 - upper))
+
+        @pl.when(k == STEPS - 1)
+        def _():
+            taken(far, k, 1 - upper)
+
+        @pl.when(k > 0)
+        def _():
+            finish_other([(k - 1, 1 - upper)])
+
+        taken(near, k, 0)
+        finish((k, upper))
+
+        @pl.when(k == STEPS - 1)
+        def _():
+            finish((k, 1 - upper))
+
+        finish_other([(k, upper)])
+        return carry
+
+    def arrive_inner(k, carry):
+        taken(near, k, 0)
+
+        @pl.when(k < STEPS - 2)
+        def _():
+            taken(far, k + 1, 1 - upper, (3, outward))
+
+        @pl.when(k == STEPS - 2)
+        def _():
+            taken(far, k + 1, 1 - upper, (3, outward), arrays=(1,))
+            taken(far, k + 1, 1 - upper, arrays=(0,))
+
+        @pl.when(k == STEPS - 1)
+        def _():
+            finish_other(finish((k, 0)))
             taken(near, k, 1)
-
-        @pl.when(is_end)
-        def _():
-            @pl.when(k > 0)
+            finish_other(finish((k, 1)))
+
+        @pl.when(k < STEPS - 1)
+        def _():
+            taken(near, k, 1)
+            done = finish((k, 0), (k, 1))
+
+            @pl.when(k < STEPS - 2)
             def _():
-                taken(far, k - 1, upper)
-
-            taken(near, k, 0)
-
-            @pl.when(k > 0)
-            def _():
-                taken(far, k - 1, 1 - upper)
-
-        @pl.when(is_inner)
-        def _():
-            taken(far, k, upper, (2, inward), (3, outward))
-
-            @pl.when(k > 0)
-            def _():
-                taken(near, k - 1, 1)
-
-            taken(near, k, 0)
-
-        @pl.when(jnp.logical_and(is_inner, k < STEPS - 1))
-        def _():
-            taken(far, k, 1 - upper, (3, outward))
-
-        @pl.when(jnp.logical_and(is_inner, k == STEPS - 1))
-        def _():
-            taken(near, k, 1)
-            taken(far, k, 1 - upper)
-
-        @pl.when(k > 0)
-        def _():
-            finish(k - 1)
+                taken(far, k + 2, upper, (2, inward), (3, outward))
+
+            finish_other(done)
 
         return carry
-
-    lax.fori_loop(0, STEPS, arrive, 0)
 
     @pl.when(is_end)
     def _():
-        taken(far, STEPS - 1, upper)
-        taken(far, STEPS - 1, 1 - upper)
-
-    finish(STEPS - 1)
+        lax.fori_loop(0, STEPS, arrive_end, 0)
+        finish_other([(STEPS - 1, 1 - upper)])
+
+    @pl.when(is_inner)
+    def _():
+        taken(far, 0, upper, (2, inward), (3, outward))
+        taken(far, 1, upper, (2, inward), (3, outward))
+        taken(far, 0, 1 - upper, (3, outward))
+        lax.fori_loop(0, STEPS, arrive_inner, 0)
+
     for copy in c_sends:
         copy.wait_recv()
 
@@ -384,7 +415,7 @@
         halves[i].start()
 
     def spread(n):
-        for d in range(1, n_ep):
+        for d in far + near:
             p = peer_of(ep, d, n_ep)
             copy = remote(
                 second.at[n, p], second_in.at[n, ep], s2.at[n, d - 1], r2.at[n, d - 1], p, tp
@@ -544,16 +575,18 @@
             third.at[0], final_in.at[slot], s4.at[0], r4.at[slot], ep, across
         )
 
-    high, low = gather_tokens(own + 1), gather_tokens(own)
+    high = gather_tokens(own + 1)
     side_copy.wait_recv()
     high = high + final_in[2 * (pairs - 1)].astype(F32)
     for m in range(pairs - 1):
+        final_copy(2 * m + 1).wait_recv()
+        high = high + final_in[2 * m + 1].astype(F32)
+    out[:, split:] = high.astype(BF16)
+    low = gather_tokens(own)
+    for m in range(pairs - 1):
         final_copy(2 * m).wait_recv()
         low = low + final_in[2 * m].astype(F32)
-        final_copy(2 * m + 1).wait_recv()
-        high = high + final_in[2 * m + 1].astype(F32)
     out[:, :split] = low.astype(BF16)
-    out[:, split:] = high.astype(BF16)
 
     def drained(ref, slot):
         remote(ref, ref, drain.at[slot], drain.at[slot], ep, sibling).wait_send()
@@ -562,16 +595,16 @@
     def _():
         drained(sends.at[:, : len(near)], 0)
         if far:
-            drained(sends.at[:, : len(far), :, :chunk], 1)
-        drained(rows_v.at[:, : len(near), :, : half // 2 - chunk], 2)
+            drained(sends.at[0, : len(far), :, :chunk], 1)
+        drained(rows_v.at[0, : len(near), :, : half - chunk], 2)
 
     @pl.when(is_inner)
     def _():
         drained(sends.at[:, : n_ep - 1, :, : half // 2], 0)
-        drained(sends.at[:, : len(near), :, :chunk], 1)
+        drained(sends.at[0, : len(near), :, :chunk], 1)
         if far:
             drained(rows_v.at[:, : len(far), :, : half // 2], 2)
-            drained(rows_v.at[:, : len(far), :, : half - chunk], 3)
+            drained(rows_v.at[0, : len(far), :, : model - chunk], 3)
 
     drained(rows_v.at[:, : n_ep - 1, :, :half], 4)
     for copy in c_sends + sc_sends + tot_sends + list(halves.values()) + list(moves.values()):

time: 78.6 us -> 77.4 us (0.985)
  Pallas kernels: 77.8 us -> 76.4 us
    pallas_call x1, Pallas kernels: 74.9 us -> 73.6 us  [layer(): pl.pallas_call(functools.partial(layer_kernel, n_ep, n_tp, cap), out_shap...]
where the time goes in v3:
time: 77.4 us; the launch traced here: 77.2 us
  Pallas kernels  76.4 us (99%)
  between operations  0.8 us (1%)
    pallas_call x1, Pallas kernels, layer(): pl.pallas_call(functools.partial(layer_kernel, n_ep, n_tp, cap), out_shap...  73.6 us
    pallas_call x1, Pallas kernels, deliver(): pl.pallas_call(functools.partial(deliver_kernel, count), out_shape=tuple(...  2.85 us

profile of v3, /device:TPU:0, one launch (start us, length us, event | category | flops | bytes accessed | tf_op | source)
XLA Modules:
  0.0 77.2 jit_solution(10478693195245549246)
XLA Ops:
  0.6 73.6 %shard_map.127 = (bf16[256,512]{1,0:T(8,128)(2,1)S(1)}, f32[1,256]{1,0:T(1,128)S(1)}, f32[2,256]{1,0:T(2,128)S(1)}, bf16[4096,256]{1,0:T(8,128)(2,1)S(1)}, bf16[...) custom-call(s32[2,256]{1,0:T(2,128)} %bitcast.14, f32[1,256]{1,0:T(1,128)} %bitcast.16, f32[2,256]{1,0:T(2,128)} %bitcast.15, ...), custom_call_target="tpu_custom_call" | custom-call | tf_op jit(solution)/shard_map/pallas_call | solution.py:635
  74.2 2.8 %shard_map.128 = (bf16[256,512]{1,0:T(8,128)(2,1)}, f32[1,256]{1,0:T(1,128)}, f32[2,256]{1,0:T(2,128)}, bf16[4096,256]{1,0:T(8,128)(2,1)}, bf16[4096,256]{1,0:T(8,128)(2,1)}, /*index=5*/bf16[256,4096]{1,0:T(8,128)(2,1)}) custom-call(bf16[256,512]{1,0:T(8,128)(2,1)S(1)} %get-tuple-element.18.refs_0_, f32[1,256]{1,0:T(1,128)S(1)} %get-tuple-element.19.refs_1_, ...), custom_call_target="tpu_custom_call" | custom-call | tf_op jit(solution)/shard_map/pallas_call | solution.py:711

commit v4 on v3

--- a/solution.py
+++ b/solution.py
@@ -383,8 +383,8 @@
         ggu[part, :units] = (weighted * up * sig * (1.0 + gate * (1.0 - sig))).astype(BF16)
         ggu[part, units:] = (weighted * silu).astype(BF16)
 
-    def partial(share):
-        part = pl.ds(pl.multiple_of(share * width, width), width)
+    def partial(share, offset=0, size=width):
+        part = pl.ds(pl.multiple_of(share * width + offset, size), size)
         return dot_nt(ggu[:, :units], wg[part, :]) + dot_nt(ggu[:, units:], wu[part, :])
 
     sc_sends = []
@@ -446,11 +446,29 @@
             spread(side)
             spread(own + 1)
 
-    for i in range(nz):
-        give_half(i)
-        if i:
-            join(i - 1)
-    join(nz - 1)
+    def lead_part(h):
+        return pl.ds(h * split, split)
+
+    for h in range(2):
+        first[0, :, lead_part(h)] = partial(
+            2 * order[0] + 1 - core, h * split, split
+        ).astype(BF16)
+        halves[0, h] = remote(
+            first.at[0, :, lead_part(h)], first_in.at[0, :, lead_part(h)],
+            s1.at[h * nz], r1.at[h * nz], ep, sibling,
+        )
+        halves[0, h].start()
+    for h in range(2):
+        total = partial(2 * order[0] + core, h * split, split)
+        halves[0, h].wait_recv()
+        total = total + first_in[0, :, lead_part(h)].astype(F32)
+        second[h] = total.astype(BF16).reshape(second.shape[1:])
+        spread(h)
+    give_half(1)
+    for i in range(1, nz):
+        if i < nz - 1:
+            give_half(i + 1)
+        join(i)
 
     def tile(t):
         return pl.ds(pl.multiple_of(t * width, width), width)
@@ -683,7 +701,7 @@
             dma((n_ep - 1,)), dma((n_ep - 1,)),
             dma((n_tp - 1,)), dma((n_tp - 1,)),
             dma((n_ep - 1,)), dma((n_ep - 1,)),
-            dma((nz,)), dma((nz,)),
+            dma((nz + 1,)), dma((nz + 1,)),
             dma((2 * nz - 1, n_ep - 1)), dma((2 * nz - 1, n_ep - 1)),
             dma((2 * nz - 4,)), dma((2 * nz - 4,)),
             dma((2 * nz - 3,)), dma((nz - 1,)),

time: 77.4 us -> 77.1 us (level)
  no operation moved by 1% of the time
where the time goes in v4:
time: 77.1 us; the launch traced here: 76.9 us
  Pallas kernels  76.1 us (99%)
  between operations  0.8 us (1%)
    pallas_call x1, Pallas kernels, layer(): pl.pallas_call(functools.partial(layer_kernel, n_ep, n_tp, cap), out_shap...  73.2 us
    pallas_call x1, Pallas kernels, deliver(): pl.pallas_call(functools.partial(deliver_kernel, count), out_shape=tuple(...  2.85 us

profile of v4, /device:TPU:0, one launch (start us, length us, event | category | flops | bytes accessed | tf_op | source)
XLA Modules:
  0.0 76.9 jit_solution(14532994011529660013)
XLA Ops:
  0.6 73.2 %shard_map.127 = (bf16[256,512]{1,0:T(8,128)(2,1)S(1)}, f32[1,256]{1,0:T(1,128)S(1)}, f32[2,256]{1,0:T(2,128)S(1)}, bf16[4096,256]{1,0:T(8,128)(2,1)S(1)}, bf16[...) custom-call(s32[2,256]{1,0:T(2,128)} %bitcast.14, f32[1,256]{1,0:T(1,128)} %bitcast.16, f32[2,256]{1,0:T(2,128)} %bitcast.15, ...), custom_call_target="tpu_custom_call" | custom-call | tf_op jit(solution)/shard_map/pallas_call | solution.py:653
  73.9 2.8 %shard_map.128 = (bf16[256,512]{1,0:T(8,128)(2,1)}, f32[1,256]{1,0:T(1,128)}, f32[2,256]{1,0:T(2,128)}, bf16[4096,256]{1,0:T(8,128)(2,1)}, bf16[4096,256]{1,0:T(8,128)(2,1)}, /*index=5*/bf16[256,4096]{1,0:T(8,128)(2,1)}) custom-call(bf16[256,512]{1,0:T(8,128)(2,1)S(1)} %get-tuple-element.18.refs_0_, f32[1,256]{1,0:T(1,128)S(1)} %get-tuple-element.19.refs_1_, ...), custom_call_target="tpu_custom_call" | custom-call | tf_op jit(solution)/shard_map/pallas_call | solution.py:729

commit v5 on v4

--- a/solution.py
+++ b/solution.py
@@ -368,6 +368,22 @@
     for copy in c_sends:
         copy.wait_recv()
 
+    def partial(share, offset=0, size=width, own=slice(None)):
+        part = pl.ds(pl.multiple_of(share * width + offset, size), size)
+        return dot_nt(ggu[own, :units], wg[part, :]) + dot_nt(ggu[own, units:], wu[part, :])
+
+    pairs, pair = nz // 2, z // 2
+    owners = []
+    for m in range(1, pairs):
+        them = peer_of(pair, m, pairs)
+        odd = lax.rem(them, 2)
+        owners += [(m, 2 * them + odd), (m, 2 * them + 1 - odd)]
+    n_far = 2 * len(owners)
+    side, own = n_far, n_far + 1
+    order = [q for _, q in owners[:1]] + [2 * pair + 1 - lax.rem(z, 2)]
+    order += [q for _, q in owners[1:]] + [z]
+    split = width // 2
+
     for p in range(n_ep):
         part = pl.ds(p * cap, cap)
         weight = jnp.broadcast_to(c_in[p], (LANES, capp)).T[:cap, :1]
@@ -382,10 +398,7 @@
         hid[part, :] = (weight * hidden).astype(BF16)
         ggu[part, :units] = (weighted * up * sig * (1.0 + gate * (1.0 - sig))).astype(BF16)
         ggu[part, units:] = (weighted * silu).astype(BF16)
-
-    def partial(share, offset=0, size=width):
-        part = pl.ds(pl.multiple_of(share * width + offset, size), size)
-        return dot_nt(ggu[:, :units], wg[part, :]) + dot_nt(ggu[:, units:], wu[part, :])
+        first[0, part, :] = partial(2 * order[0] + 1 - core, own=part).astype(BF16)
 
     sc_sends = []
     for k in range(1, n_tp):
@@ -396,17 +409,6 @@
         copy.start()
         sc_sends.append(copy)
 
-    pairs, pair = nz // 2, z // 2
-    owners = []
-    for m in range(1, pairs):
-        them = peer_of(pair, m, pairs)
-        odd = lax.rem(them, 2)
-        owners += [(m, 2 * them + odd), (m, 2 * them + 1 - odd)]
-    n_far = 2 * len(owners)
-    side, own = n_far, n_far + 1
-    order = [q for _, q in owners[:1]] + [2 * pair + 1 - lax.rem(z, 2)]
-    order += [q for _, q in owners[1:]] + [z]
-    split = width // 2
     halves, moves = {}, {}
 
     def give_half(i):
@@ -450,9 +452,6 @@
         return pl.ds(h * split, split)
 
     for h in range(2):
-        first[0, :, lead_part(h)] = partial(
-            2 * order[0] + 1 - core, h * split, split
-        ).astype(BF16)
         halves[0, h] = remote(
             first.at[0, :, lead_part(h)], first_in.at[0, :, lead_part(h)],
             s1.at[h * nz], r1.at[h * nz], ep, sibling,

time: 77.1 us -> 77.3 us (level)
  no operation moved by 1% of the time
where the time goes in v5:
time: 77.3 us; the launch traced here: 77 us
  Pallas kernels  76.2 us (99%)
  between operations  0.8 us (1%)
    pallas_call x1, Pallas kernels, layer(): pl.pallas_call(functools.partial(layer_kernel, n_ep, n_tp, cap), out_shap...  73.4 us
    pallas_call x1, Pallas kernels, deliver(): pl.pallas_call(functools.partial(deliver_kernel, count), out_shape=tuple(...  2.85 us

profile of v5, /device:TPU:0, one launch (start us, length us, event | category | flops | bytes accessed | tf_op | source)
XLA Modules:
  0.0 77.0 jit_solution(6948123295748120351)
XLA Ops:
  0.6 73.4 %shard_map.127 = (bf16[256,512]{1,0:T(8,128)(2,1)S(1)}, f32[1,256]{1,0:T(1,128)S(1)}, f32[2,256]{1,0:T(2,128)S(1)}, bf16[4096,256]{1,0:T(8,128)(2,1)S(1)}, bf16[...) custom-call(s32[2,256]{1,0:T(2,128)} %bitcast.14, f32[1,256]{1,0:T(1,128)} %bitcast.16, f32[2,256]{1,0:T(2,128)} %bitcast.15, ...), custom_call_target="tpu_custom_call" | custom-call | tf_op jit(solution)/shard_map/pallas_call | solution.py:652
  74.0 2.8 %shard_map.128 = (bf16[256,512]{1,0:T(8,128)(2,1)}, f32[1,256]{1,0:T(1,128)}, f32[2,256]{1,0:T(2,128)}, bf16[4096,256]{1,0:T(8,128)(2,1)}, bf16[4096,256]{1,0:T(8,128)(2,1)}, /*index=5*/bf16[256,4096]{1,0:T(8,128)(2,1)}) custom-call(bf16[256,512]{1,0:T(8,128)(2,1)S(1)} %get-tuple-element.18.refs_0_, f32[1,256]{1,0:T(1,128)S(1)} %get-tuple-element.19.refs_1_, ...), custom_call_target="tpu_custom_call" | custom-call | tf_op jit(solution)/shard_map/pallas_call | solution.py:728
